TPU v7x, 32 devices: a whole 2x2x4 slice. The times are simulated.
32 devices in a mesh: sp: 16 (over z, x, core), tp: 2 (over y).
Axes of the slice: x: 2, y: 2, z: 4, core: 2. Of those that a mesh axis runs over, the one named last changes fastest.
Arguments:
- stream: bfloat16 [4096, 2048], P('sp'), may hold values from -6 to 6
- doc_ids: int32 [4096], P('sp'), may hold values from 0 to 3, never falling along the last dimension, each value on 1 to 2048 neighbouring positions
- norm_gain: float32 [2, 2048], replicated, may hold values from 0.1 to 1.9
- w_query: bfloat16 [2, 2048, 1024], P(None, None, 'tp'), may hold values from -0.125 to 0.125
- w_key: bfloat16 [2, 2048, 1024], P(None, None, 'tp'), may hold values from -0.125 to 0.125
- w_value: bfloat16 [2, 2048, 1024], P(None, None, 'tp'), may hold values from -0.125 to 0.125
- query_gain: float32 [2, 64], replicated, may hold values from 0.4 to 7
- key_gain: float32 [2, 64], replicated, may hold values from 0.4 to 7
- offset_bias: float32 [2, 16, 8, 16], P(None, 'tp'), may hold values from -4 to 4
- w_output: bfloat16 [2, 1024, 2048], replicated, may hold values from -0.1875 to 0.1875
Outputs:
- result: bfloat16 [4096, 2048], P('sp')
Inputs may be any that keep to these rules, and one draw needn't show every extreme that they name: `doc_ids`: numbers never fall along the sequence; each document holds 1 to 2048 positions and one holds exactly 2048.
All inputs are finite; a program needn't handle non-finite values.
Results may differ from a plain program's by a relative error of at most 0.034.
The roundings to bfloat16 on the way count: a program that leaves them out, or rounds other values in their place, can miss the bound.
Values may be sent and summed in bfloat16 or wider, within the bound.
A program may use at most 128 MiB of HBM per device.

v0:
```python
import jax
import jax.numpy as jnp
from jax import lax
from jax.sharding import PartitionSpec as P

HEAD_DIM = 64
GRID_W = 64
WIN_ROWS = 8
WIN_COLS = 16


eps = 1e-06


def padded(block, sides, width):
    for axis, dim in sides:
        count = lax.axis_size(axis)
        forward = [(i, i + 1) for i in range(count - 1)]
        backward = [(target, source) for source, target in forward]
        low = lax.ppermute(
            lax.slice_in_dim(block, block.shape[dim] - width, None, axis=dim), axis, forward
        )
        high = lax.ppermute(lax.slice_in_dim(block, 0, width, axis=dim), axis, backward)
        block = jnp.concatenate([low, block, high], axis=dim)
    return block


def head_norm(raw_rows, gain_row):
    split_rows = raw_rows.reshape(raw_rows.shape[0], -1, HEAD_DIM)
    inverse = lax.rsqrt(jnp.mean(split_rows * split_rows, axis=-1, keepdims=True) + eps)
    return (split_rows * inverse * gain_row).astype(jnp.bfloat16).reshape(raw_rows.shape)


def project(layer_params, row_block):
    gain_vector, query_weight, key_weight, value_weight, query_scale, key_scale = layer_params
    token_rows = row_block.astype(jnp.float32)
    inv_rms = lax.rsqrt(jnp.mean(token_rows * token_rows, axis=-1, keepdims=True) + eps)
    normed = (token_rows * inv_rms * gain_vector).astype(jnp.bfloat16)
    queries = head_norm(
        jnp.dot(normed, query_weight, preferred_element_type=jnp.float32), query_scale
    )
    key_rows = head_norm(jnp.dot(normed, key_weight, preferred_element_type=jnp.float32), key_scale)
    value_rows = jnp.dot(normed, value_weight, preferred_element_type=jnp.float32).astype(
        jnp.bfloat16
    )
    return jnp.concatenate([queries, key_rows, value_rows], axis=1)


def offset_table(head_bias):
    key_reach = 2 * WIN_COLS - 1
    offsets = (
        jnp.arange(key_reach, dtype=jnp.int32)[None, :]
        - jnp.arange(WIN_COLS, dtype=jnp.int32)[:, None]
    )
    inside = (offsets >= 0) & (offsets < WIN_COLS)
    one_hot = (offsets[:, :, None] == jnp.arange(WIN_COLS, dtype=jnp.int32)[None, None, :]).astype(
        jnp.float32
    )
    lookup = jnp.einsum("hjc,qkc->qhjk", head_bias, one_hot, precision=lax.Precision.HIGHEST)
    return (lookup, inside)


def window_attend(queries, pair_pad, query_marks, mark_pad, head_bias):
    heads_here = head_bias.shape[0]
    tokens_here = queries.shape[0]
    grid_rows = tokens_here // GRID_W
    col_blocks = GRID_W // WIN_COLS
    key_reach = 2 * WIN_COLS - 1
    margin = WIN_COLS // 2
    col_pad = ((0, 0), (margin, WIN_COLS - 1 - margin))
    pair_grid = jnp.pad(pair_pad.reshape(grid_rows + WIN_ROWS, GRID_W, -1), col_pad + ((0, 0),))
    mark_grid = jnp.pad(mark_pad.reshape(grid_rows + WIN_ROWS, GRID_W), col_pad)
    pair_band = jnp.stack(
        [pair_grid[row_shift : row_shift + grid_rows] for row_shift in range(WIN_ROWS)], axis=1
    )
    mark_band = jnp.stack(
        [mark_grid[row_shift : row_shift + grid_rows] for row_shift in range(WIN_ROWS)], axis=1
    )
    pair_win = jnp.stack(
        [
            pair_band[:, :, col_block * WIN_COLS : col_block * WIN_COLS + key_reach]
            for col_block in range(col_blocks)
        ],
        axis=2,
    )
    mark_win = jnp.stack(
        [
            mark_band[:, :, col_block * WIN_COLS : col_block * WIN_COLS + key_reach]
            for col_block in range(col_blocks)
        ],
        axis=2,
    )
    pair_win = pair_win.reshape(grid_rows, WIN_ROWS, col_blocks, key_reach, 2, heads_here, HEAD_DIM)
    key_win = pair_win[:, :, :, :, 0]
    value_win = pair_win[:, :, :, :, 1]
    query_grid = queries.reshape(grid_rows, col_blocks, WIN_COLS, heads_here, HEAD_DIM)
    scores = jnp.einsum(
        "rbqhd,rjbkhd->rbqhjk", query_grid, key_win, preferred_element_type=jnp.float32
    )
    lookup, inside = offset_table(head_bias)
    own_marks = query_marks.reshape(grid_rows, col_blocks, WIN_COLS)
    same_doc = mark_win.transpose(0, 2, 1, 3)[:, :, None, :, :] == own_marks[:, :, :, None, None]
    allowed = same_doc & inside[None, None, :, None, :]
    scores = scores * HEAD_DIM ** (-0.5) + lookup[None, None]
    scores = jnp.where(allowed[:, :, :, None], scores, -jnp.inf)
    highest = jnp.max(scores, axis=(4, 5), keepdims=True)
    shifted_exp = jnp.exp(scores - highest)
    weights = (shifted_exp / jnp.sum(shifted_exp, axis=(4, 5), keepdims=True)).astype(jnp.bfloat16)
    mixed = jnp.einsum(
        "rbqhjk,rjbkhd->rbqhd", weights, value_win, preferred_element_type=jnp.float32
    )
    return mixed.astype(jnp.bfloat16).reshape(tokens_here, heads_here * HEAD_DIM)


def attend(projected, marks, head_bias):
    head_width = projected.shape[1] // 3
    halo_tokens = WIN_ROWS // 2 * GRID_W
    pair_pad, mark_pad = (
        padded(projected[:, head_width:], (("sp", 0),), halo_tokens),
        padded(marks, (("sp", 0),), halo_tokens),
    )
    return window_attend(projected[:, :head_width], pair_pad, marks, mark_pad, head_bias)


def on_device(
    stream, doc_ids, norm_gain, w_query, w_key, w_value, query_gain, key_gain, offset_bias, w_output
):
    marks = (doc_ids + 1).astype(jnp.bfloat16)
    layer_count = w_query.shape[0]
    current = stream
    for layer_index in range(layer_count):
        layer_params = (
            norm_gain[layer_index],
            w_query[layer_index],
            w_key[layer_index],
            w_value[layer_index],
            query_gain[layer_index],
            key_gain[layer_index],
        )
        attended = attend(project(layer_params, current), marks, offset_bias[layer_index])
        every_head = lax.all_gather(attended, "tp", axis=1, tiled=True)
        projected = jnp.dot(every_head, w_output[layer_index], preferred_element_type=jnp.float32)
        current = (current.astype(jnp.float32) + projected).astype(jnp.bfloat16)
    return current


def solution(mesh):
    return jax.shard_map(
        on_device,
        mesh=mesh,
        in_specs=(
            P("sp", None),
            P("sp"),
            P(),
            P(None, None, "tp"),
            P(None, None, "tp"),
            P(None, None, "tp"),
            P(),
            P(),
            P(None, "tp", None, None),
            P(),
        ),
        out_specs=P("sp", None),
        check_vma=False,
    )
```

profile of v0, /device:TPU:10, one launch (start us, length us, event | category | flops | bytes accessed | tf_op | source)
XLA Modules:
  0.0 237.8 jit_solution(1758482249919251222)
XLA Ops:
  0.8 1.5 fusion.38
  2.3 3.9 %slice_bitcast_fusion.9 = (bf16[512,2048]{0,1:T(8,128)(2,1)S(1)}, bf16[512,2048]{0,1:T(8,128)(2,1)}) fusion(bf16[2,2048,512]{2,1,0:T(8,128)(2,1)} %param.14), kind=kLoop, calls=%fused_computation.66 | loop fusion | bytes 8388608 | tf_op jit(solution)/shard_map/dot_general | solution.py:42
  6.2 4.0 %copy.68 = bf16[512,2048]{1,0:T(8,128)(2,1)} copy(bf16[512,2048]{0,1:T(8,128)(2,1)} %get-tuple-element.16) | data formatting | bytes 4194304 | tf_op jit(solution)/shard_map/dot_general | solution.py:42
  10.2 2.4 %multiply_reduce_fusion.3 = (f32[256,8]{0,1:T(8,128)S(1)}, f32[256,8,64]{0,2,1:T(8,128)S(1)}) fusion(bf16[8,64,2048]{2,1,0:T(8,128)(2,1)} %bitcast.333, f32[2048]{0:T(1024)S(1)} %bitcast.341, f32[256]{0:T(256)S(1)} %add_rsqrt_fusion.5, bf16[256,2048]{1,0:T(8,128)(2,1)S(1)} %copy-done.8), kind=kOutput, calls=%fused_computation.150 | convolution fusion | flops 539228160 | bytes 3687424 | tf_op jit(solution)/shard_map/dot_general | solution.py:42
  13.0 2.8 %fusion.56 = bf16[256,512]{1,0:T(8,128)(2,1)S(1)} fusion(bf16[2,2048,512]{2,1,0:T(8,128)(2,1)} %param.15, bf16[256,2048]{1,0:T(8,128)(2,1)} %param.10, f32[2048]{0:T(1024)S(1)} %bitcast.342, f32[256]{0:T(256)S(1)} %add_rsqrt_fusion.5), kind=kOutput, calls=%fused_computation.96 | convolution fusion | flops 539099136 | bytes 3417088 | tf_op jit(solution)/shard_map/dot_general | solution.py:43
  16.7 1.9 collective-permute-start
  18.6 3.6 %collective-permute-start.1 = (bf16[256,1024]{1,0:T(8,128)(2,1)}, bf16[256,1024]{1,0:T(8,128)(2,1)}, u32[]{:S(2)}, u32[]{:S(2)}) collective-permute-start(bf16[256,1024]{1,0:T(8,128)(2,1)} %pad_maximum_fusion.2), channel_id=1, source_target_pairs={{2,0},{4,2},{6,4},{8,6},{10,8},{12,10},{14,12},{16,14},{18,16},{20... | collective-permute-start | bytes 1572872 | tf_op jit(solution)/shard_map/ppermute | solution.py:23
  22.3 1.9 collective-permute-start.2
  24.2 3.6 %collective-permute-start.3 = (bf16[256]{0:T(256)(128)(2,1)S(1)}, bf16[256]{0:T(256)(128)(2,1)S(1)}, u32[]{:S(2)}, u32[]{:S(2)}) collective-permute-start(bf16[256]{0:T(256)(128)(2,1)S(1)} %add_convert_fusion), channel_id=1, source_target_pairs={{2,0},{4,2},{6,4},{8,6},{10,8},{12,10},{14,12},{16,14},{18,16},{20... | collective-permute-start | bytes 1544 | tf_op jit(solution)/shard_map/ppermute | solution.py:23
  29.4 2.2 slice_bitcast_fusion.8
  31.6 4.2 %copy.79 = bf16[512,2048]{1,0:T(8,128)(2,1)} copy(bf16[512,2048]{0,1:T(8,128)(2,1)} %get-tuple-element.14) | data formatting | bytes 4194304 | tf_op jit(solution)/shard_map/dot_general | solution.py:40
  35.8 2.8 %multiply_reduce_fusion.2 = (f32[256,8]{0,1:T(8,128)S(1)}, f32[256,8,64]{0,2,1:T(8,128)S(1)}) fusion(bf16[8,64,2048]{2,1,0:T(8,128)(2,1)} %bitcast.332, f32[2048]{0:T(1024)S(1)} %bitcast.343, f32[256]{0:T(256)S(1)} %add_rsqrt_fusion.5, bf16[256,2048]{1,0:T(8,128)(2,1)} %param.10), kind=kOutput, calls=%fused_computation.148 | convolution fusion | flops 539228160 | bytes 3687424 | tf_op jit(solution)/shard_map/dot_general | solution.py:40
  41.1 2.5 %copy.84 = bf16[512,2048]{1,0:T(8,128)(2,1)} copy(bf16[512,2048]{0,1:T(8,128)(2,1)S(1)} %get-tuple-element.15) | data formatting | bytes 4194304 | tf_op jit(solution)/shard_map/dot_general | solution.py:42
  43.5 4.0 %copy.94 = bf16[512,2048]{1,0:T(8,128)(2,1)} copy(bf16[512,2048]{0,1:T(8,128)(2,1)} %get-tuple-element.13) | data formatting | bytes 4194304 | tf_op jit(solution)/shard_map/dot_general | solution.py:40
  48.7 1.3 pad_maximum_fusion
  50.6 3.0 %fusion.130 = (bf16[4,8,31,1024]{3,2,0,1:T(8,128)(2,1)S(1)}, bf16[4,8,31,1024]{3,2,0,1:T(8,128)(2,1)}, bf16[4,8,31,1024]{3,2,0,1:T(8,128)(2,1)}, bf16[4,8,31,1024]{3,2,0,1:T(8,128)(2,1)}) fusion(bf16[4,8,79,1024]{3,2,0,1:T(8,128)(2,1)S(1)} %fusion.85), kind=kLoop, calls=%fused_computation.206 | loop fusion | bytes 16252928 | tf_op jit(solution)/shard_map/slice | solution.py:81
  53.6 6.2 %reshape.154 = bf16[4,8,1,31,2,8,64]{6,5,4,3,0,1,2:T(8,128)(2,1)} reshape(bf16[4,8,31,1024]{3,2,0,1:T(8,128)(2,1)} %get-tuple-element.12) | data formatting | bytes 4063232 | tf_op jit(solution)/shard_map/stack | solution.py:79
  59.8 5.2 %copy_dynamic-update-slice_fusion.7 = bf16[4,8,4,31,2,8,64]{6,3,1,5,2,0,4:T(8,128)(2,1)} fusion(bf16[4,8,1,31,2,8,64]{6,5,4,3,0,1,2:T(8,128)(2,1)} %reshape.154), kind=kLoop, calls=%fused_computation.31 | loop fusion | bytes 6225920
  65.0 6.2 %reshape.155 = bf16[4,8,1,31,2,8,64]{6,5,4,3,0,1,2:T(8,128)(2,1)} reshape(bf16[4,8,31,1024]{3,2,0,1:T(8,128)(2,1)} %get-tuple-element.11) | data formatting | bytes 4063232 | tf_op jit(solution)/shard_map/stack | solution.py:79
  71.2 6.2 %reshape.156 = bf16[4,8,1,31,2,8,64]{6,5,4,3,0,1,2:T(8,128)(2,1)} reshape(bf16[4,8,31,1024]{3,2,0,1:T(8,128)(2,1)} %get-tuple-element.10) | data formatting | bytes 4063232 | tf_op jit(solution)/shard_map/stack | solution.py:79
  77.4 3.9 %reshape.157 = bf16[4,8,1,31,2,8,64]{6,5,4,3,0,1,2:T(8,128)(2,1)} reshape(bf16[4,8,31,1024]{3,2,0,1:T(8,128)(2,1)S(1)} %get-tuple-element.9) | data formatting | bytes 4063232 | tf_op jit(solution)/shard_map/stack | solution.py:79
  81.2 5.3 %copy_dynamic-update-slice_fusion.6 = bf16[4,8,4,31,2,8,64]{6,3,1,5,2,0,4:T(8,128)(2,1)} fusion(bf16[4,8,4,31,2,8,64]{6,3,1,5,2,0,4:T(8,128)(2,1)} %copy_dynamic-update-slice_fusion.7, bf16[4,8,1,31,2,8,64]{6,5,4,3,0,1,2:T(8,128)(2,1)} %reshape.155), kind=kLoop, calls=%fused_computation.30 | loop fusion | bytes 8257536
  86.6 3.0 %copy_dynamic-update-slice_fusion.5 = bf16[4,8,4,31,2,8,64]{6,3,1,5,2,0,4:T(8,128)(2,1)} fusion(bf16[4,8,4,31,2,8,64]{6,3,1,5,2,0,4:T(8,128)(2,1)} %copy_dynamic-update-slice_fusion.6, bf16[4,8,1,31,2,8,64]{6,5,4,3,0,1,2:T(8,128)(2,1)S(1)} %copy-done), kind=kLoop, calls=%fused_computation.29 | loop fusion | bytes 6225920
  89.6 3.0 %copy_dynamic-update-slice_fusion.4 = bf16[4,8,4,31,2,8,64]{6,3,1,5,2,0,4:T(8,128)(2,1)} fusion(bf16[4,8,4,31,2,8,64]{6,3,1,5,2,0,4:T(8,128)(2,1)} %copy_dynamic-update-slice_fusion.5, bf16[4,8,1,31,2,8,64]{6,5,4,3,0,1,2:T(8,128)(2,1)S(1)} %copy-done.1), kind=kLoop, calls=%fused_computation.28 | loop fusion | bytes 6225920 | tf_op jit(solution)/shard_map/stack | solution.py:79
  92.6 13.9 %fusion.8 = (f32[4,4,16,8]{2,3,1,0:T(8,128)S(1)}, f32[4,4,8,8,31,16]{4,5,3,2,1,0:T(8,128)S(1)}) fusion(f32[16,8,8,31]{3,0,2,1:T(8,128)} %copy.82, pred[4,4,16,8,31]{4,2,3,1,0:T(8,128)(4,1)S(1)} %compare_and_fusion, bf16[4,4,16,8,64,1]{4,3,2,1,0,5:T(8,128)(2,1)} %bitcast.336, bf16[4,8,4,31,2,8,64]{6,3,1,5,2,0,4:T(8,128)(2,1)} %copy_dynamic-update-slice_fusion.4), kind=kOutput, calls=%fused_computation.18 | convolution fusion | flops 67041280 | bytes 11540480 | tf_op jit(solution)/shard_map/rbqhd,rjbkhd->rbqhjk/dot_general | solution.py:97
  106.5 3.9 %fusion.6 = f32[4,4,16,8]{2,3,1,0:T(8,128)S(1)} fusion(f32[4,4,8,8,31,16]{4,5,3,2,1,0:T(8,128)S(1)} %get-tuple-element.32, f32[4,4,16,8]{2,3,1,0:T(8,128)S(1)} %get-tuple-element.31, f32[16,8,8,31]{3,0,2,1:T(8,128)} %copy.82, pred[4,4,16,8,31]{4,2,3,1,0:T(8,128)(4,1)S(1)} %compare_and_fusion), kind=kLoop, calls=%fused_computation.16 | loop fusion | flops 2537472 | bytes 2238464 | tf_op jit(solution)/shard_map/reduce_sum | solution.py:108
  110.5 10.3 %fusion.54 = bf16[4,4,16,8,64]{4,2,3,1,0:T(8,128)(2,1)S(1)} fusion(f32[4,4,8,8,31,16]{4,5,3,2,1,0:T(8,128)S(1)} %get-tuple-element.32, f32[4,4,16,8]{2,3,1,0:T(8,128)S(1)} %fusion.6, f32[4,4,16,8]{2,3,1,0:T(8,128)S(1)} %get-tuple-element.31, f32[16,8,8,31]{3,0,2,1:T(8,128)S(1)} %copy-done.5, pred[4,4,16,8,31]{4,2,3,1,0:T(8,128)(4,1)S(1)} %compare_and_fusion, ...), kind=kOutput, calls=%fused_computation.94 | convolution fusion | flops 68190208 | bytes 10889216 | tf_op jit(solution)/shard_map/rbqhjk,rjbkhd->rbqhd/dot_general | solution.py:109
  121.2 9.7 %all_gather.6 = bf16[256,1024]{1,0:T(8,128)(2,1)S(1)} all-gather(bf16[256,512]{1,0:T(8,128)(2,1)S(1)} %reshape.141), channel_id=1, replica_groups=mesh['sp'=16,'tp'=2] {'tp'}, dimensions={1}, use_global_device_ids=true | all-gather | bytes 786432 | tf_op jit(solution)/shard_map/all_gather | solution.py:141
  131.0 4.1 %fusion.41 = (f32[256]{0:T(256)S(1)}, bf16[256,2048]{1,0:T(8,128)(2,1)S(1)}) fusion(bf16[256,1024]{1,0:T(8,128)(2,1)S(1)} %all_gather.6, bf16[2,1024,2048]{2,1,0:T(8,128)(2,1)} %param.19, bf16[256,2048]{1,0:T(8,128)(2,1)} %param.10), kind=kOutput, calls=%fused_computation.57 | convolution fusion | flops 1076887296 | bytes 6816768 | tf_op jit(solution)/shard_map/dot_general | solution.py:142
  138.2 1.9 collective-permute-start.4
  140.1 3.6 %collective-permute-start.5 = (bf16[256,1024]{1,0:T(8,128)(2,1)S(1)}, bf16[256,1024]{1,0:T(8,128)(2,1)}, u32[]{:S(2)}, u32[]{:S(2)}) collective-permute-start(bf16[256,1024]{1,0:T(8,128)(2,1)S(1)} %pad_maximum_fusion.3), channel_id=1, source_target_pairs={{2,0},{4,2},{6,4},{8,6},{10,8},{12,10},{14,12},{16,14},{18,16},{20... | collective-permute-start | bytes 1572872 | tf_op jit(solution)/shard_map/ppermute | solution.py:23
  143.8 2.8 %multiply_reduce_fusion = (f32[256,8]{0,1:T(8,128)S(1)}, f32[256,8,64]{0,2,1:T(8,128)S(1)}) fusion(bf16[8,64,2048]{2,1,0:T(8,128)(2,1)} %bitcast.330, f32[2048]{0:T(1024)S(1)} %bitcast.340, f32[256]{0:T(256)S(1)} %add_rsqrt_fusion.4, bf16[256,2048]{1,0:T(8,128)(2,1)} %copy-done.14), kind=kOutput, calls=%fused_computation.144 | convolution fusion | flops 539228160 | bytes 3687424 | tf_op jit(solution)/shard_map/dot_general | solution.py:40
  147.7 6.6 %collective-permute-done.4 = bf16[256,1024]{1,0:T(8,128)(2,1)S(1)} collective-permute-done((bf16[256,1024]{1,0:T(8,128)(2,1)S(1)}, bf16[256,1024]{1,0:T(8,128)(2,1)S(1)}, u32[]{:S(2)}, u32[]{:S(2)}) %collective-permute-start.4) | collective-permute-done | bytes 524320 | tf_op jit(solution)/shard_map/ppermute | solution.py:20
  154.3 1.2 pad_maximum_fusion.1
  156.1 3.3 %fusion.129 = (bf16[4,8,31,1024]{3,2,0,1:T(8,128)(2,1)S(1)}, bf16[4,8,31,1024]{3,2,0,1:T(8,128)(2,1)}, bf16[4,8,31,1024]{3,2,0,1:T(8,128)(2,1)}, bf16[4,8,31,1024]{3,2,0,1:T(8,128)(2,1)}) fusion(bf16[4,8,79,1024]{3,2,0,1:T(8,128)(2,1)S(1)} %fusion.101), kind=kLoop, calls=%fused_computation.205 | loop fusion | bytes 16252928 | tf_op jit(solution)/shard_map/slice | solution.py:81
  159.4 6.2 %reshape.158 = bf16[4,8,1,31,2,8,64]{6,5,4,3,0,1,2:T(8,128)(2,1)} reshape(bf16[4,8,31,1024]{3,2,0,1:T(8,128)(2,1)} %get-tuple-element.8) | data formatting | bytes 4063232 | tf_op jit(solution)/shard_map/stack | solution.py:79
  165.6 5.2 %copy_dynamic-update-slice_fusion.3 = bf16[4,8,4,31,2,8,64]{6,3,1,5,2,0,4:T(8,128)(2,1)} fusion(bf16[4,8,1,31,2,8,64]{6,5,4,3,0,1,2:T(8,128)(2,1)} %reshape.158), kind=kLoop, calls=%fused_computation.25 | loop fusion | bytes 6225920
  170.8 6.2 %reshape.159 = bf16[4,8,1,31,2,8,64]{6,5,4,3,0,1,2:T(8,128)(2,1)} reshape(bf16[4,8,31,1024]{3,2,0,1:T(8,128)(2,1)} %get-tuple-element.7) | data formatting | bytes 4063232 | tf_op jit(solution)/shard_map/stack | solution.py:79
  177.0 6.2 %reshape.160 = bf16[4,8,1,31,2,8,64]{6,5,4,3,0,1,2:T(8,128)(2,1)} reshape(bf16[4,8,31,1024]{3,2,0,1:T(8,128)(2,1)} %get-tuple-element.6) | data formatting | bytes 4063232 | tf_op jit(solution)/shard_map/stack | solution.py:79
  183.2 3.9 %reshape.161 = bf16[4,8,1,31,2,8,64]{6,5,4,3,0,1,2:T(8,128)(2,1)} reshape(bf16[4,8,31,1024]{3,2,0,1:T(8,128)(2,1)S(1)} %get-tuple-element.5) | data formatting | bytes 4063232 | tf_op jit(solution)/shard_map/stack | solution.py:79
  187.1 5.3 %copy_dynamic-update-slice_fusion.2 = bf16[4,8,4,31,2,8,64]{6,3,1,5,2,0,4:T(8,128)(2,1)} fusion(bf16[4,8,4,31,2,8,64]{6,3,1,5,2,0,4:T(8,128)(2,1)} %copy_dynamic-update-slice_fusion.3, bf16[4,8,1,31,2,8,64]{6,5,4,3,0,1,2:T(8,128)(2,1)} %reshape.159), kind=kLoop, calls=%fused_computation.24 | loop fusion | bytes 8257536
  192.4 3.0 %copy_dynamic-update-slice_fusion.1 = bf16[4,8,4,31,2,8,64]{6,3,1,5,2,0,4:T(8,128)(2,1)} fusion(bf16[4,8,4,31,2,8,64]{6,3,1,5,2,0,4:T(8,128)(2,1)} %copy_dynamic-update-slice_fusion.2, bf16[4,8,1,31,2,8,64]{6,5,4,3,0,1,2:T(8,128)(2,1)S(1)} %copy-done.2), kind=kLoop, calls=%fused_computation.23 | loop fusion | bytes 6225920
  195.4 3.0 %copy_dynamic-update-slice_fusion = bf16[4,8,4,31,2,8,64]{6,3,1,5,2,0,4:T(8,128)(2,1)} fusion(bf16[4,8,4,31,2,8,64]{6,3,1,5,2,0,4:T(8,128)(2,1)} %copy_dynamic-update-slice_fusion.1, bf16[4,8,1,31,2,8,64]{6,5,4,3,0,1,2:T(8,128)(2,1)S(1)} %copy-done.3), kind=kLoop, calls=%fused_computation.22 | loop fusion | bytes 6225920 | tf_op jit(solution)/shard_map/stack | solution.py:79
  198.4 13.6 %fusion.9 = (f32[4,4,16,8]{2,3,1,0:T(8,128)S(1)}, f32[4,4,8,8,31,16]{4,5,3,2,1,0:T(8,128)S(1)}) fusion(f32[16,8,8,31]{3,0,2,1:T(8,128)S(1)} %copy.97, pred[4,4,16,8,31]{4,2,3,1,0:T(8,128)(4,1)S(1)} %compare_and_fusion, bf16[4,4,16,8,64,1]{4,3,2,1,0,5:T(8,128)(2,1)} %bitcast.337, bf16[4,8,4,31,2,8,64]{6,3,1,5,2,0,4:T(8,128)(2,1)} %copy_dynamic-update-slice_fusion), kind=kOutput, calls=%fused_computation.19 | convolution fusion | flops 67041280 | bytes 11143168 | tf_op jit(solution)/shard_map/rbqhd,rjbkhd->rbqhjk/dot_general | solution.py:97
  212.1 3.0 %fusion.7 = f32[4,4,16,8]{2,3,1,0:T(8,128)S(1)} fusion(f32[4,4,8,8,31,16]{4,5,3,2,1,0:T(8,128)S(1)} %get-tuple-element.40, f32[4,4,16,8]{2,3,1,0:T(8,128)S(1)} %get-tuple-element.39, f32[16,8,8,31]{3,0,2,1:T(8,128)S(1)} %copy.97, pred[4,4,16,8,31]{4,2,3,1,0:T(8,128)(4,1)S(1)} %compare_and_fusion), kind=kLoop, calls=%fused_computation.17 | loop fusion | flops 2537472 | bytes 2238464 | tf_op jit(solution)/shard_map/reduce_sum | solution.py:108
  215.1 10.3 %fusion.55 = bf16[4,4,16,8,64]{4,2,3,1,0:T(8,128)(2,1)S(1)} fusion(f32[4,4,8,8,31,16]{4,5,3,2,1,0:T(8,128)S(1)} %get-tuple-element.40, f32[4,4,16,8]{2,3,1,0:T(8,128)S(1)} %fusion.7, f32[4,4,16,8]{2,3,1,0:T(8,128)S(1)} %get-tuple-element.39, f32[16,8,8,31]{3,0,2,1:T(8,128)S(1)} %copy.97, pred[4,4,16,8,31]{4,2,3,1,0:T(8,128)(4,1)S(1)} %compare_and_fusion, ...), kind=kOutput, calls=%fused_computation.95 | convolution fusion | flops 68190208 | bytes 10889216 | tf_op jit(solution)/shard_map/rbqhjk,rjbkhd->rbqhd/dot_general | solution.py:109
  225.8 7.1 %all_gather.7 = bf16[256,1024]{1,0:T(8,128)(2,1)S(1)} all-gather(bf16[256,512]{1,0:T(8,128)(2,1)S(1)} %reshape.144), channel_id=1, replica_groups=mesh['sp'=16,'tp'=2] {'tp'}, dimensions={1}, use_global_device_ids=true | all-gather | bytes 786432 | tf_op jit(solution)/shard_map/all_gather | solution.py:141
  232.9 4.7 %fusion.35 = bf16[256,2048]{1,0:T(8,128)(2,1)} fusion(bf16[256,1024]{1,0:T(8,128)(2,1)S(1)} %all_gather.7, bf16[2,1024,2048]{2,1,0:T(8,128)(2,1)} %param.19, bf16[256,2048]{1,0:T(8,128)(2,1)} %copy-done.14), kind=kOutput, calls=%fused_computation.53 | convolution fusion | flops 1075314688 | bytes 6815744 | tf_op jit(solution)/shard_map/dot_general | solution.py:142
  (100 shorter events, 13.3 us)
Async XLA Ops:
  6.2 4.0 %copy-start.8 = (bf16[256,2048]{1,0:T(8,128)(2,1)S(1)}, bf16[256,2048]{1,0:T(8,128)(2,1)}, u32[]{:S(2)}) copy-start(bf16[256,2048]{1,0:T(8,128)(2,1)} %param.10) | copy-start | bytes 3145732
  6.2 6.5 %copy-start.10 = (f32[2,64]{1,0:T(2,128)S(1)}, f32[2,64]{1,0:T(2,128)}, u32[]{:S(2)}) copy-start(f32[2,64]{1,0:T(2,128)} %param.17) | copy-start | bytes 1540
  12.7 9.6 %copy-start.13 = (s32[256]{0:T(256)S(1)}, s32[256]{0:T(256)}, u32[]{:S(2)}) copy-start(s32[256]{0:T(256)} %param.11) | copy-start | bytes 3076
  12.7 15.2 %copy-start.9 = (f32[2,8,8,16]{3,2,1,0:T(8,128)S(1)}, f32[2,8,8,16]{3,2,1,0:T(8,128)}, u32[]{:S(2)}) copy-start(f32[2,8,8,16]{3,2,1,0:T(8,128)} %param.18) | copy-start | bytes 24580
  13.0 16.4 %copy-start.4 = (bf16[2,2048,512]{2,1,0:T(8,128)(2,1)S(1)}, bf16[2,2048,512]{2,1,0:T(8,128)(2,1)}, u32[]{:S(2)}) copy-start(bf16[2,2048,512]{2,1,0:T(8,128)(2,1)} %param.13) | copy-start | bytes 12582916
  16.7 32.0 %collective-permute-start = (bf16[256,1024]{1,0:T(8,128)(2,1)}, bf16[256,1024]{1,0:T(8,128)(2,1)}, u32[]{:S(2)}, u32[]{:S(2)}) collective-permute-start(bf16[256,1024]{1,0:T(8,128)(2,1)} %pad_maximum_fusion.2), channel_id=1, source_target_pairs={{0,2},{2,4},{4,6},{6,8},{8,10},{10,12},{12,14},{14,16},{16,18},{18... | collective-permute-start | bytes 1572872 | tf_op jit(solution)/shard_map/ppermute | solution.py:20
  18.6 30.1 %collective-permute-start.1 = (bf16[256,1024]{1,0:T(8,128)(2,1)}, bf16[256,1024]{1,0:T(8,128)(2,1)}, u32[]{:S(2)}, u32[]{:S(2)}) collective-permute-start(bf16[256,1024]{1,0:T(8,128)(2,1)} %pad_maximum_fusion.2), channel_id=1, source_target_pairs={{2,0},{4,2},{6,4},{8,6},{10,8},{12,10},{14,12},{16,14},{18,16},{20... | collective-permute-start | bytes 1572872 | tf_op jit(solution)/shard_map/ppermute | solution.py:23
  22.3 25.6 %collective-permute-start.2 = (bf16[256]{0:T(256)(128)(2,1)S(1)}, bf16[256]{0:T(256)(128)(2,1)S(1)}, u32[]{:S(2)}, u32[]{:S(2)}) collective-permute-start(bf16[256]{0:T(256)(128)(2,1)S(1)} %add_convert_fusion), channel_id=1, source_target_pairs={{0,2},{2,4},{4,6},{6,8},{8,10},{10,12},{12,14},{14,16},{16,18},{18... | collective-permute-start | bytes 1544 | tf_op jit(solution)/shard_map/ppermute | solution.py:20
  24.2 23.7 %collective-permute-start.3 = (bf16[256]{0:T(256)(128)(2,1)S(1)}, bf16[256]{0:T(256)(128)(2,1)S(1)}, u32[]{:S(2)}, u32[]{:S(2)}) collective-permute-start(bf16[256]{0:T(256)(128)(2,1)S(1)} %add_convert_fusion), channel_id=1, source_target_pairs={{2,0},{4,2},{6,4},{8,6},{10,8},{12,10},{14,12},{16,14},{18,16},{20... | collective-permute-start | bytes 1544 | tf_op jit(solution)/shard_map/ppermute | solution.py:23
  31.6 6.9 %copy-start.11 = (f32[2,64]{1,0:T(2,128)S(1)}, f32[2,64]{1,0:T(2,128)}, u32[]{:S(2)}) copy-start(f32[2,64]{1,0:T(2,128)} %param.16) | copy-start | bytes 1540
  43.5 4.0 %copy-start.7 = (f32[16,8,8,31]{3,2,1,0:T(8,128)S(1)}, f32[16,8,8,31]{3,2,1,0:T(8,128)}, u32[]{:S(2)}) copy-start(f32[16,8,8,31]{3,2,1,0:T(8,128)} %convolution_bitcast_fusion) | copy-start | bytes 380932
  81.2 5.3 %copy-start = (bf16[4,8,1,31,2,8,64]{6,5,4,3,0,1,2:T(8,128)(2,1)S(1)}, bf16[4,8,1,31,2,8,64]{6,5,4,3,0,1,2:T(8,128)(2,1)}, u32[]{:S(2)}) copy-start(bf16[4,8,1,31,2,8,64]{6,5,4,3,0,1,2:T(8,128)(2,1)} %reshape.156) | copy-start | bytes 6094852
  86.6 3.0 %copy-start.1 = (bf16[4,8,1,31,2,8,64]{6,5,4,3,0,1,2:T(8,128)(2,1)S(1)}, bf16[4,8,1,31,2,8,64]{6,5,4,3,0,1,2:T(8,128)(2,1)}, u32[]{:S(2)}) copy-start(bf16[4,8,1,31,2,8,64]{6,5,4,3,0,1,2:T(8,128)(2,1)} %reshape.157) | copy-start | bytes 6094852
  106.5 3.9 %copy-start.5 = (f32[16,8,8,31]{3,0,2,1:T(8,128)S(1)}, f32[16,8,8,31]{3,0,2,1:T(8,128)}, u32[]{:S(2)}) copy-start(f32[16,8,8,31]{3,0,2,1:T(8,128)} %copy.82) | copy-start | bytes 380932
  131.0 4.1 %copy-start.12 = (bf16[2,2048,512]{2,1,0:T(8,128)(2,1)S(1)}, bf16[2,2048,512]{2,1,0:T(8,128)(2,1)}, u32[]{:S(2)}) copy-start(bf16[2,2048,512]{2,1,0:T(8,128)(2,1)} %param.15) | copy-start | bytes 12582916
  135.0 2.8 %copy-start.14 = (bf16[256,2048]{1,0:T(8,128)(2,1)}, bf16[256,2048]{1,0:T(8,128)(2,1)S(1)}, u32[]{:S(2)}) copy-start(bf16[256,2048]{1,0:T(8,128)(2,1)S(1)} %get-tuple-element.34) | copy-start | bytes 3145732
  135.0 2.0 copy-start.6
  138.2 16.1 %collective-permute-start.4 = (bf16[256,1024]{1,0:T(8,128)(2,1)S(1)}, bf16[256,1024]{1,0:T(8,128)(2,1)S(1)}, u32[]{:S(2)}, u32[]{:S(2)}) collective-permute-start(bf16[256,1024]{1,0:T(8,128)(2,1)S(1)} %pad_maximum_fusion.3), channel_id=1, source_target_pairs={{0,2},{2,4},{4,6},{6,8},{8,10},{10,12},{12,14},{14,16},{16,18},{18... | collective-permute-start | bytes 1572872 | tf_op jit(solution)/shard_map/ppermute | solution.py:20
  140.1 14.2 %collective-permute-start.5 = (bf16[256,1024]{1,0:T(8,128)(2,1)S(1)}, bf16[256,1024]{1,0:T(8,128)(2,1)}, u32[]{:S(2)}, u32[]{:S(2)}) collective-permute-start(bf16[256,1024]{1,0:T(8,128)(2,1)S(1)} %pad_maximum_fusion.3), channel_id=1, source_target_pairs={{2,0},{4,2},{6,4},{8,6},{10,8},{12,10},{14,12},{16,14},{18,16},{20... | collective-permute-start | bytes 1572872 | tf_op jit(solution)/shard_map/ppermute | solution.py:23
  187.1 5.3 %copy-start.2 = (bf16[4,8,1,31,2,8,64]{6,5,4,3,0,1,2:T(8,128)(2,1)S(1)}, bf16[4,8,1,31,2,8,64]{6,5,4,3,0,1,2:T(8,128)(2,1)}, u32[]{:S(2)}) copy-start(bf16[4,8,1,31,2,8,64]{6,5,4,3,0,1,2:T(8,128)(2,1)} %reshape.160) | copy-start | bytes 6094852
  192.4 3.0 %copy-start.3 = (bf16[4,8,1,31,2,8,64]{6,5,4,3,0,1,2:T(8,128)(2,1)S(1)}, bf16[4,8,1,31,2,8,64]{6,5,4,3,0,1,2:T(8,128)(2,1)}, u32[]{:S(2)}) copy-start(bf16[4,8,1,31,2,8,64]{6,5,4,3,0,1,2:T(8,128)(2,1)} %reshape.161) | copy-start | bytes 6094852
where the time goes:
time: 243 us; the launch traced here: 238 us
  local copies, waits for them, and re-layouts  113 us (47%)
  matrix products  70.8 us (29%)
  blocking collectives  16.8 us (7%)
  starting transfers between devices  16.7 us (7%)
  other arithmetic  12.8 us (5%)
  waiting for transfers between devices  6.58 us (3%)
    another operation x10, local copies, waits for them, and re-layouts, window_attend(): jnp.stack([pair_band[:, :, col_block * WIN_COLS:col_block * WIN_COLS + ke...  51 us
    unnamed x57, local copies, waits for them, and re-layouts  29.3 us
    dot_general x2, matrix products, window_attend(): jnp.einsum('rbqhd,rjbkhd->rbqhjk', query_grid, key_win, preferred_element...  27.5 us
    dot_general x2, matrix products, window_attend(): jnp.einsum('rbqhjk,rjbkhd->rbqhd', weights, value_win, preferred_element_...  20.6 us
    all_gather x2, blocking collectives, on_device(): every_head = lax.all_gather(attended, 'tp', axis=1, tiled=True)  16.8 us
    ppermute x3, starting transfers between devices, padded(): lax.ppermute(lax.slice_in_dim(block, 0, width, axis=dim), axis, backward)  10.9 us
    dot_general x3, local copies, waits for them, and re-layouts, project(): jnp.dot(normed, query_weight, preferred_element_type=jnp.float32)  10.4 us
    dot_general x3, local copies, waits for them, and re-layouts, project(): jnp.dot(normed, key_weight, preferred_element_type=jnp.float32)  10.3 us
  transfers between devices with their start and end apart: 6, of which 1 were waited for; matrix products, arithmetic and copies ran while one was open for 10% of the time, Pallas kernels for 0%

commit v1 on v0

v1 whole, which is shorter than its diff:
```python
import functools

import jax
import jax.numpy as jnp
from jax import lax
from jax.experimental import pallas as pl
from jax.experimental.pallas import tpu as pltpu
from jax.sharding import PartitionSpec as P

HEAD_DIM = 64
GRID_W = 64
WIN_ROWS = 8
WIN_COLS = 16
EPS = 1e-06
LOW = WIN_ROWS // 2 * GRID_W
HIGH = (WIN_ROWS - WIN_ROWS // 2 - 1) * GRID_W
KEYS = WIN_ROWS * GRID_W
NEG = -1e30
MESH = pl.DeviceIdType.MESH
F32 = jnp.float32
BF16 = jnp.bfloat16


def kernel(
    sp_size,
    tp_size,
    stream_ref,
    doc_ref,
    norm_gain_ref,
    wq_hbm,
    wk_hbm,
    wv_hbm,
    q_gain_ref,
    k_gain_ref,
    bias_ref,
    wo_hbm,
    out_ref,
    wbuf,
    wobuf,
    hbuf,
    nbuf,
    qbuf,
    kbuf,
    vbuf,
    att,
    acc,
    table,
    maskbuf,
    marks,
    w_sem,
    wo_sem,
    mark_send,
    mark_recv,
    k_send,
    k_recv,
    v_send,
    v_recv,
    a_send,
    a_recv,
):
    layers, width, head_width = wk_hbm.shape
    tokens = stream_ref.shape[0]
    rows = tokens // GRID_W
    group = min(128, head_width)
    per_group = group // HEAD_DIM
    groups = head_width // group
    me = lax.axis_index("sp")
    mine = lax.axis_index("tp")
    has_prev = me > 0
    has_next = me < sp_size - 1
    prev = lax.rem(me + sp_size - 1, sp_size)
    following = lax.rem(me + 1, sp_size)

    def w_copy(layer, which):
        source = (wq_hbm, wk_hbm, wv_hbm)[which]
        return pltpu.make_async_copy(
            source.at[layer], wbuf.at[layer, which], w_sem.at[layer, which]
        )

    def wo_copy(layer):
        return pltpu.make_async_copy(wo_hbm.at[layer], wobuf.at[layer], wo_sem.at[layer])

    w_copy(0, 1).start()
    w_copy(0, 2).start()

    barrier = pltpu.get_barrier_semaphore()

    @pl.when(has_prev)
    def _():
        pl.semaphore_signal(barrier, inc=1, device_id={"sp": prev}, device_id_type=MESH)

    @pl.when(has_next)
    def _():
        pl.semaphore_signal(barrier, inc=1, device_id={"sp": following}, device_id_type=MESH)

    for step in range(1, tp_size):
        pl.semaphore_signal(
            barrier,
            inc=1,
            device_id={"tp": lax.rem(mine + step, tp_size)},
            device_id_type=MESH,
        )

    def halo(buf, layer, send, recv):
        here = buf.at[layer]
        ahead = pltpu.make_async_remote_copy(
            src_ref=here.at[pl.ds(LOW + tokens - LOW, LOW)],
            dst_ref=here.at[pl.ds(0, LOW)],
            send_sem=send.at[layer, 0],
            recv_sem=recv.at[layer, 0],
            device_id={"sp": following},
            device_id_type=MESH,
        )
        back = pltpu.make_async_remote_copy(
            src_ref=here.at[pl.ds(LOW, HIGH)],
            dst_ref=here.at[pl.ds(LOW + tokens, HIGH)],
            send_sem=send.at[layer, 1],
            recv_sem=recv.at[layer, 1],
            device_id={"sp": prev},
            device_id_type=MESH,
        )
        return ahead, back

    def mark_copies():
        ahead = pltpu.make_async_remote_copy(
            src_ref=doc_ref,
            dst_ref=marks.at[0],
            send_sem=mark_send.at[0],
            recv_sem=mark_recv.at[0],
            device_id={"sp": following},
            device_id_type=MESH,
        )
        back = pltpu.make_async_remote_copy(
            src_ref=doc_ref,
            dst_ref=marks.at[1],
            send_sem=mark_send.at[1],
            recv_sem=mark_recv.at[1],
            device_id={"sp": prev},
            device_id_type=MESH,
        )
        return ahead, back

    def start_both(pair):
        @pl.when(has_next)
        def _():
            pair[0].start()

        @pl.when(has_prev)
        def _():
            pair[1].start()

    def wait_send_both(pair):
        @pl.when(has_next)
        def _():
            pair[0].wait_send()

        @pl.when(has_prev)
        def _():
            pair[1].wait_send()

    def wait_low(pair):
        @pl.when(has_prev)
        def _():
            pair[0].wait_recv()

    def wait_high(pair):
        @pl.when(has_next)
        def _():
            pair[1].wait_recv()

    def att_copy(layer, row, step):
        block = att.at[layer, mine, pl.ds(row * GRID_W, GRID_W)]
        return pltpu.make_async_remote_copy(
            src_ref=block,
            dst_ref=block,
            send_sem=a_send.at[layer, step - 1, row],
            recv_sem=a_recv.at[layer, step - 1, row],
            device_id={"tp": lax.rem(mine + step, tp_size)},
            device_id_type=MESH,
        )

    @pl.when(jnp.logical_not(has_prev))
    def _():
        marks[0] = jnp.full((1, tokens), -1, jnp.int32)
        kbuf[:, 0:LOW, :] = jnp.zeros((layers, LOW, head_width), BF16)
        vbuf[:, 0:LOW, :] = jnp.zeros((layers, LOW, head_width), BF16)

    @pl.when(jnp.logical_not(has_next))
    def _():
        marks[1] = jnp.full((1, tokens), -1, jnp.int32)
        kbuf[:, LOW + tokens :, :] = jnp.zeros((layers, HIGH, head_width), BF16)
        vbuf[:, LOW + tokens :, :] = jnp.zeros((layers, HIGH, head_width), BF16)

    span = min(256, head_width)
    head_row = lax.broadcasted_iota(jnp.int32, (span, span), 0) // HEAD_DIM
    head_col = lax.broadcasted_iota(jnp.int32, (span, span), 1) // HEAD_DIM
    averager = jnp.where(head_row == head_col, 1.0 / HEAD_DIM, 0.0).astype(BF16)

    def head_norm(raw, gain):
        squares = raw * raw
        coarse = squares.astype(BF16)
        fine = (squares - coarse.astype(F32)).astype(BF16)
        mean = jnp.dot(coarse, averager, preferred_element_type=F32) + jnp.dot(
            fine, averager, preferred_element_type=F32
        )
        return (raw * lax.rsqrt(mean + EPS) * gain).astype(BF16)

    def project(layer, which, write):
        for start in range(0, head_width, span):
            write(
                start,
                jnp.dot(
                    nbuf[...],
                    wbuf[layer, which, :, start : start + span],
                    preferred_element_type=F32,
                ),
            )

    def build_tables():
        query_col = lax.broadcasted_iota(jnp.int32, (GRID_W, 128), 0)
        key_col = lax.rem(lax.broadcasted_iota(jnp.int32, (GRID_W, 128), 1), GRID_W)
        offset = key_col - query_col + WIN_COLS // 2
        band = (offset >= 0) & (offset < WIN_COLS)
        heads = head_width // HEAD_DIM
        tiles = KEYS // 128
        for layer in range(layers):
            for head in range(heads):
                for tile in range(tiles):
                    index = (layer * heads + head) * tiles + tile
                    line = jnp.broadcast_to(bias_ref[index : index + 1, :], (GRID_W, 128))
                    line = pltpu.roll(line, 128 - WIN_COLS // 2, 1, stride=1, stride_axis=0)
                    table[
                        layer,
                        head * GRID_W : (head + 1) * GRID_W,
                        tile * 128 : (tile + 1) * 128,
                    ] = jnp.where(band, line, NEG)

    def build_masks():
        own = doc_ref[...]
        every = jnp.concatenate([marks[0], own, marks[1]], axis=1).astype(F32)
        own_rows = jnp.broadcast_to(own.astype(F32), (128, tokens)).T
        base = tokens - LOW
        for row in range(rows):
            left = base + row * GRID_W
            keys_here = every[:, left : left + KEYS]
            queries_here = own_rows[row * GRID_W : (row + 1) * GRID_W, 0:1]
            maskbuf[row] = jnp.where(queries_here == keys_here, 0.0, NEG)

    lane = lax.broadcasted_iota(jnp.int32, (GRID_W, group), 1)

    def attend_row(layer, row):
        low = row * GRID_W
        for g in range(groups):
            cols = slice(g * group, (g + 1) * group)
            q = qbuf[low : low + GRID_W, cols]
            if per_group == 2:
                zero = jnp.zeros_like(q)
                q = jnp.concatenate(
                    [
                        jnp.where(lane < HEAD_DIM, q, zero),
                        jnp.where(lane >= HEAD_DIM, q, zero),
                    ],
                    axis=0,
                )
            k = kbuf[layer, low : low + KEYS, cols]
            v = vbuf[layer, low : low + KEYS, cols]
            scores = lax.dot_general(
                q, k, (((1,), (1,)), ((), ())), preferred_element_type=F32
            )
            exps, sums = [], []
            for i in range(per_group):
                head = g * per_group + i
                s = (
                    scores[i * GRID_W : (i + 1) * GRID_W]
                    + table[layer, head * GRID_W : (head + 1) * GRID_W, :]
                    + maskbuf[row]
                )
                e = jnp.exp(s - jnp.max(s, axis=-1, keepdims=True))
                sums.append(jnp.sum(e, axis=-1, keepdims=True))
                exps.append(e.astype(BF16))
            weights = exps[0] if per_group == 1 else jnp.concatenate(exps, axis=0)
            mixed = jnp.dot(weights, v, preferred_element_type=F32)
            parts = [
                mixed[i * GRID_W : (i + 1) * GRID_W] / sums[i] for i in range(per_group)
            ]
            result = (
                parts[0] if per_group == 1 else jnp.where(lane < HEAD_DIM, parts[0], parts[1])
            )
            att[layer, mine, low : low + GRID_W, cols] = result.astype(BF16)

    chunk = 512
    for layer in range(layers):
        source = stream_ref if layer == 0 else hbuf
        target = out_ref if layer == layers - 1 else hbuf

        block = 32

        def norm_rows(i, carry):
            at = pl.ds(pl.multiple_of(i * block, block), block)
            x = source[at, :].astype(F32)
            inverse = lax.rsqrt(jnp.mean(x * x, axis=-1, keepdims=True) + EPS)
            nbuf[at, :] = (x * inverse * norm_gain_ref[layer : layer + 1, :]).astype(BF16)
            return carry

        lax.fori_loop(0, tokens // block, norm_rows, 0)

        k_gain = k_gain_ref[layer : layer + 1, :]
        q_gain = q_gain_ref[layer : layer + 1, :] * HEAD_DIM ** (-0.5)

        w_copy(layer, 1).wait()
        if layer == 0:
            w_copy(0, 0).start()
            wo_copy(0).start()

        def write_k(start, raw):
            kbuf[layer, LOW : LOW + tokens, start : start + span] = head_norm(
                raw, k_gain[:, start : start + span]
            )

        project(layer, 1, write_k)
        if layer == 0:
            degree = has_prev.astype(jnp.int32) + has_next.astype(jnp.int32) + (tp_size - 1)
            pl.semaphore_wait(barrier, degree)
            start_both(mark_copies())
        start_both(halo(kbuf, layer, k_send, k_recv))

        w_copy(layer, 2).wait()

        def write_v(start, raw):
            vbuf[layer, LOW : LOW + tokens, start : start + span] = raw.astype(BF16)

        project(layer, 2, write_v)
        start_both(halo(vbuf, layer, v_send, v_recv))
        if layer == 0:
            for later in range(1, layers):
                for which in (1, 2, 0):
                    w_copy(later, which).start()
                wo_copy(later).start()

        w_copy(layer, 0).wait()

        def write_q(start, raw):
            qbuf[:, start : start + span] = head_norm(raw, q_gain[:, start : start + span])

        project(layer, 0, write_q)
        if layer == 0:
            build_tables()
            wait_low(mark_copies())
            wait_high(mark_copies())
            build_masks()

        wait_low(halo(kbuf, layer, k_send, k_recv))
        wait_low(halo(vbuf, layer, v_send, v_recv))
        for row in range(rows):
            if row == 1:
                wait_high(halo(kbuf, layer, k_send, k_recv))
                wait_high(halo(vbuf, layer, v_send, v_recv))
            attend_row(layer, row)
            for step in range(1, tp_size):
                att_copy(layer, row, step).start()

        wo_copy(layer).wait()

        def out_part(owner, start):
            return jnp.dot(
                att[layer, owner],
                wobuf[
                    layer,
                    pl.ds(pl.multiple_of(owner * head_width, head_width), head_width),
                    start : start + chunk,
                ],
                preferred_element_type=F32,
            )

        for start in range(0, width, chunk):
            cols = slice(start, start + chunk)
            acc[:, cols] = source[:, cols].astype(F32) + out_part(mine, start)
        for step in range(1, tp_size):
            for row in range(rows):
                att_copy(layer, row, step).wait_recv()
            owner = lax.rem(mine + tp_size - step, tp_size)
            for start in range(0, width, chunk):
                cols = slice(start, start + chunk)
                total = acc[:, cols] + out_part(owner, start)
                if step == tp_size - 1:
                    target[:, cols] = total.astype(BF16)
                else:
                    acc[:, cols] = total
        if tp_size == 1:
            target[...] = acc[...].astype(BF16)

    wait_send_both(mark_copies())
    for layer in range(layers):
        wait_send_both(halo(kbuf, layer, k_send, k_recv))
        wait_send_both(halo(vbuf, layer, v_send, v_recv))
        for step in range(1, tp_size):
            for row in range(rows):
                att_copy(layer, row, step).wait_send()


def on_device(
    sp_size,
    tp_size,
    stream,
    doc_ids,
    norm_gain,
    w_query,
    w_key,
    w_value,
    query_gain,
    key_gain,
    offset_bias,
    w_output,
):
    tokens, width = stream.shape
    layers, _, head_width = w_query.shape
    heads = head_width // HEAD_DIM
    rows = tokens // GRID_W
    all_width = w_output.shape[1]
    bias = jnp.pad(offset_bias, ((0, 0), (0, 0), (0, 0), (0, GRID_W - WIN_COLS)))
    bias = bias.reshape(layers * heads * (KEYS // 128), 128)
    vmem = pl.BlockSpec(memory_space=pltpu.VMEM)
    hbm = pl.BlockSpec(memory_space=pl.ANY)
    sem = pltpu.SemaphoreType.DMA
    peers = max(1, tp_size - 1)
    return pl.pallas_call(
        functools.partial(kernel, sp_size, tp_size),
        out_shape=jax.ShapeDtypeStruct((tokens, width), BF16),
        in_specs=[vmem, vmem, vmem, hbm, hbm, hbm, vmem, vmem, vmem, hbm],
        out_specs=vmem,
        scratch_shapes=[
            pltpu.VMEM((layers, 3, width, head_width), BF16),
            pltpu.VMEM((layers, all_width, width), BF16),
            pltpu.VMEM((tokens, width), BF16),
            pltpu.VMEM((tokens, width), BF16),
            pltpu.VMEM((tokens, head_width), BF16),
            pltpu.VMEM((layers, LOW + tokens + HIGH, head_width), BF16),
            pltpu.VMEM((layers, LOW + tokens + HIGH, head_width), BF16),
            pltpu.VMEM((layers, tp_size, tokens, head_width), BF16),
            pltpu.VMEM((tokens, width), F32),
            pltpu.VMEM((layers, heads * GRID_W, KEYS), F32),
            pltpu.VMEM((rows, GRID_W, KEYS), F32),
            pltpu.VMEM((2, 1, tokens), jnp.int32),
            sem((layers, 3)),
            sem((layers,)),
            sem((2,)),
            sem((2,)),
            sem((layers, 2)),
            sem((layers, 2)),
            sem((layers, 2)),
            sem((layers, 2)),
            sem((layers, peers, rows)),
            sem((layers, peers, rows)),
        ],
        compiler_params=pltpu.CompilerParams(
            collective_id=0, has_side_effects=True, vmem_limit_bytes=60 * 1024 * 1024
        ),
    )(
        stream,
        doc_ids.reshape(1, tokens),
        norm_gain,
        w_query,
        w_key,
        w_value,
        jnp.tile(query_gain, (1, heads)),
        jnp.tile(key_gain, (1, heads)),
        bias,
        w_output,
    )


def solution(mesh):
    return jax.shard_map(
        functools.partial(on_device, mesh.shape["sp"], mesh.shape["tp"]),
        mesh=mesh,
        in_specs=(
            P("sp", None),
            P("sp"),
            P(),
            P(None, None, "tp"),
            P(None, None, "tp"),
            P(None, None, "tp"),
            P(),
            P(),
            P(None, "tp", None, None),
            P(),
        ),
        out_specs=P("sp", None),
        check_vma=False,
    )
```

time: 243 us -> 54 us (0.22); the launches traced: 238 us -> 53.7 us
  local copies, waits for them, and re-layouts: 113 us -> 6.53 us
  matrix products: 70.8 us -> 0 us
  Pallas kernels: 0 us -> 47.1 us
  blocking collectives: 16.8 us -> 0 us
  starting transfers between devices: 16.7 us -> 0 us
  other arithmetic: 12.8 us -> 0 us
  waiting for transfers between devices: 6.58 us -> 0 us
    dot_general x14 -> x0, matrix products: 70.8 us -> none  [the longest x2 27.5 us: window_attend(): jnp.einsum('rbqhd,rjbkhd->rbqhjk', query_grid, key_win, preferred_element...]
    another operation x14 -> x4, local copies, waits for them, and re-layouts: 51.3 us -> 2.69 us  [the longest x2 1.35 us: on_device(): jnp.tile(key_gain, (1, heads))]
    pallas_call x0 -> x1, Pallas kernels: none -> 47.1 us  [on_device(): pl.pallas_call(functools.partial(kernel, sp_size, tp_size), out_shape=jax...]
    unnamed x57 -> x1, local copies, waits for them, and re-layouts: 29.3 us -> 2.3 us
    dot_general x6 -> x0, local copies, waits for them, and re-layouts: 20.7 us -> none  [the longest x3 10.4 us: project(): jnp.dot(normed, query_weight, preferred_element_type=jnp.float32)]
    all_gather x2 -> x0, blocking collectives: 16.8 us -> none  [on_device(): every_head = lax.all_gather(attended, 'tp', axis=1, tiled=True)]
    ppermute x6 -> x0, starting transfers between devices: 16.7 us -> none  [the longest x3 10.9 us: padded(): lax.ppermute(lax.slice_in_dim(block, 0, width, axis=dim), axis, backward)]
    reduce_sum x3 -> x0, other arithmetic: 8.42 us -> none  [the longest x2 6.9 us: window_attend(): jnp.sum(shifted_exp, axis=(4, 5), keepdims=True)]
  transfers between devices with their start and end apart: 6 -> 0, of which waited for: 1 -> 0; matrix products, arithmetic and copies ran while one was open for 10% -> 0% of each run, Pallas kernels for 0% -> 0%
where the time goes in v1:
time: 54 us; the launch traced here: 53.7 us
  Pallas kernels  47.1 us (87%)
  local copies, waits for them, and re-layouts  6.53 us (12%)
    pallas_call x1, Pallas kernels, on_device(): pl.pallas_call(functools.partial(kernel, sp_size, tp_size), out_shape=jax...  47.1 us
    unnamed x1, local copies, waits for them, and re-layouts  2.3 us
    another operation x2, local copies, waits for them, and re-layouts, on_device(): jnp.tile(key_gain, (1, heads))  1.35 us
    another operation x2, local copies, waits for them, and re-layouts, on_device(): jnp.tile(query_gain, (1, heads))  1.34 us

profile of v1, /device:TPU:10, one launch (start us, length us, event | category | flops | bytes accessed | tf_op | source)
XLA Modules:
  0.0 53.7 jit_solution(3170232521523477742)
XLA Ops:
  0.0 0.7 %tile.8 = f32[2,8,64]{2,1,0:T(8,128)S(1)} broadcast(f32[2,64]{1,0:T(2,128)} %param.16), dimensions={0,2} | broadcast | bytes 4608 | tf_op jit(solution)/shard_map/tile | solution.py:465
  0.7 0.7 %tile.9.q_gain_ref = f32[2,512]{1,0:T(2,128)} reshape(f32[2,8,64]{2,1,0:T(8,128)S(1)} %tile.8) | data formatting | bytes 8192 | tf_op jit(solution)/shard_map/tile | solution.py:465
  1.3 0.7 %tile.20 = f32[2,8,64]{2,1,0:T(8,128)S(1)} broadcast(f32[2,64]{1,0:T(2,128)} %param.17), dimensions={0,2} | broadcast | bytes 4608 | tf_op jit(solution)/shard_map/tile | solution.py:466
  2.0 0.7 %tile.21.k_gain_ref = f32[2,512]{1,0:T(2,128)} reshape(f32[2,8,64]{2,1,0:T(8,128)S(1)} %tile.20) | data formatting | bytes 8192 | tf_op jit(solution)/shard_map/tile | solution.py:466
  2.7 0.8 %pad.4 = f32[2,8,8,64]{3,2,1,0:T(8,128)S(1)} pad(f32[2,8,8,16]{3,2,1,0:T(8,128)} %param.18, f32[]{:T(128)} %constant.2.clone.1), padding=0_0x0_0x0_0x0_48 | pad | bytes 40964 | tf_op jit(solution)/shard_map/jit(_pad)/pad | solution.py:420
  3.5 0.7 %reshape.15.bias_ref = f32[64,128]{1,0:T(8,128)} reshape(f32[2,8,8,64]{3,2,1,0:T(8,128)S(1)} %pad.4) | data formatting | bytes 65536 | tf_op jit(solution)/shard_map/reshape | solution.py:421
  4.2 47.1 %shard_map.100 = bf16[256,2048]{1,0:T(8,128)(2,1)} custom-call(bf16[256,2048]{1,0:T(8,128)(2,1)} %stream_ref.1, s32[1,256]{1,0:T(1,128)} %bitcast.3, f32[2,2048]{1,0:T(2,128)} %norm_gain_ref.1, bf16[2,2048,512]{2,1,0:T(8,128)(2,1)} %wq_hbm.1, bf16[2,2048,512]{2,1,0:T(8,128)(2,1)} %wk_hbm.1, bf16[2,2048,512]{2,1,0:T(8,128)(2,1)} %wv_hbm.1, ...), custom_call_target="tpu_custom_call" | custom-call | tf_op jit(solution)/shard_map/pallas_call | solution.py:426
  51.3 2.3 %copy.12 = bf16[256,2048]{1,0:T(8,128)(2,1)} copy(bf16[256,2048]{1,0:T(8,128)(2,1)} %shard_map.100) | data formatting | bytes 2097152

commit v2 on v1

v2 whole, which is shorter than its diff:
```python
import functools

import jax
import jax.numpy as jnp
from jax import lax
from jax.experimental import pallas as pl
from jax.experimental.pallas import tpu as pltpu
from jax.sharding import PartitionSpec as P

HEAD_DIM = 64
GRID_W = 64
WIN_ROWS = 8
WIN_COLS = 16
EPS = 1e-06
LOW = WIN_ROWS // 2 * GRID_W
HIGH = (WIN_ROWS - WIN_ROWS // 2 - 1) * GRID_W
KEYS = WIN_ROWS * GRID_W
NEG = -1e30
MESH = pl.DeviceIdType.MESH
F32 = jnp.float32
BF16 = jnp.bfloat16


def kernel(
    sp_size,
    tp_size,
    stream_ref,
    doc_ref,
    norm_gain_ref,
    wq_hbm,
    wk_hbm,
    wv_hbm,
    q_gain_ref,
    k_gain_ref,
    bias_ref,
    wo_hbm,
    out_ref,
    wqbuf,
    wkvbuf,
    wobuf,
    hbuf,
    nbuf,
    qbuf,
    kvbuf,
    att,
    acc,
    table,
    maskbuf,
    marks,
    lines,
    wq_sem,
    wkv_sem,
    wo_sem,
    mark_send,
    mark_recv,
    kv_send,
    kv_recv,
    a_send,
    a_recv,
):
    layers, width, head_width = wk_hbm.shape
    tokens = stream_ref.shape[0]
    rows = tokens // GRID_W
    group = min(128, head_width)
    per_group = group // HEAD_DIM
    groups = head_width // group
    paired = group == 128
    me = lax.axis_index("sp")
    mine = lax.axis_index("tp")
    has_prev = me > 0
    has_next = me < sp_size - 1
    prev = lax.rem(me + sp_size - 1, sp_size)
    following = lax.rem(me + 1, sp_size)

    def wq_copy(layer):
        return pltpu.make_async_copy(wq_hbm.at[layer], wqbuf.at[layer], wq_sem.at[layer])

    def wkv_copy(layer, g, part):
        source = (wk_hbm, wv_hbm)[part].at[layer]
        if paired:
            source = source.at[:, pl.ds(g * group, group)]
            target = wkvbuf.at[layer, g, :, pl.ds(part * group, group)]
        else:
            target = wkvbuf.at[layer, part]
        return pltpu.make_async_copy(source, target, wkv_sem.at[layer, g, part])

    def wo_copy(layer):
        return pltpu.make_async_copy(wo_hbm.at[layer], wobuf.at[layer], wo_sem.at[layer])

    for g in range(groups):
        for part in range(2):
            wkv_copy(0, g, part).start()

    barrier = pltpu.get_barrier_semaphore()

    @pl.when(has_prev)
    def _():
        pl.semaphore_signal(barrier, inc=1, device_id={"sp": prev}, device_id_type=MESH)

    @pl.when(has_next)
    def _():
        pl.semaphore_signal(barrier, inc=1, device_id={"sp": following}, device_id_type=MESH)

    for step in range(1, tp_size):
        pl.semaphore_signal(
            barrier,
            inc=1,
            device_id={"tp": lax.rem(mine + step, tp_size)},
            device_id_type=MESH,
        )

    def halo(layer, g):
        here = kvbuf.at[layer, g]
        ahead = pltpu.make_async_remote_copy(
            src_ref=here.at[pl.ds(tokens, LOW)],
            dst_ref=here.at[pl.ds(0, LOW)],
            send_sem=kv_send.at[layer, g, 0],
            recv_sem=kv_recv.at[layer, g, 0],
            device_id={"sp": following},
            device_id_type=MESH,
        )
        back = pltpu.make_async_remote_copy(
            src_ref=here.at[pl.ds(LOW, HIGH)],
            dst_ref=here.at[pl.ds(LOW + tokens, HIGH)],
            send_sem=kv_send.at[layer, g, 1],
            recv_sem=kv_recv.at[layer, g, 1],
            device_id={"sp": prev},
            device_id_type=MESH,
        )
        return ahead, back

    def mark_copies():
        ahead = pltpu.make_async_remote_copy(
            src_ref=doc_ref,
            dst_ref=marks.at[0],
            send_sem=mark_send.at[0],
            recv_sem=mark_recv.at[0],
            device_id={"sp": following},
            device_id_type=MESH,
        )
        back = pltpu.make_async_remote_copy(
            src_ref=doc_ref,
            dst_ref=marks.at[1],
            send_sem=mark_send.at[1],
            recv_sem=mark_recv.at[1],
            device_id={"sp": prev},
            device_id_type=MESH,
        )
        return ahead, back

    def start_both(pair):
        @pl.when(has_next)
        def _():
            pair[0].start()

        @pl.when(has_prev)
        def _():
            pair[1].start()

    def wait_send_both(pair):
        @pl.when(has_next)
        def _():
            pair[0].wait_send()

        @pl.when(has_prev)
        def _():
            pair[1].wait_send()

    def wait_low(pair):
        @pl.when(has_prev)
        def _():
            pair[0].wait_recv()

    def wait_high(pair):
        @pl.when(has_next)
        def _():
            pair[1].wait_recv()

    def att_copy(layer, g, step):
        block = att.at[layer, mine]
        if paired:
            block = block.at[:, pl.ds(g * group, group)]
        return pltpu.make_async_remote_copy(
            src_ref=block,
            dst_ref=block,
            send_sem=a_send.at[layer, step - 1, g],
            recv_sem=a_recv.at[layer, step - 1, g],
            device_id={"tp": lax.rem(mine + step, tp_size)},
            device_id_type=MESH,
        )

    @pl.when(jnp.logical_not(has_prev))
    def _():
        marks[0] = jnp.full((1, tokens), -1, jnp.int32)
        kvbuf[:, :, 0:LOW, :] = jnp.zeros((layers, groups, LOW, 2 * group), BF16)

    @pl.when(jnp.logical_not(has_next))
    def _():
        marks[1] = jnp.full((1, tokens), -1, jnp.int32)
        kvbuf[:, :, LOW + tokens :, :] = jnp.zeros((layers, groups, HIGH, 2 * group), BF16)

    span = min(256, head_width)

    def averager(size):
        head_row = lax.broadcasted_iota(jnp.int32, (size, size), 0) // HEAD_DIM
        head_col = lax.broadcasted_iota(jnp.int32, (size, size), 1) // HEAD_DIM
        return jnp.where(head_row == head_col, 1.0 / HEAD_DIM, 0.0).astype(BF16)

    def head_norm(raw, gain):
        weights = averager(raw.shape[1])
        squares = raw * raw
        coarse = squares.astype(BF16)
        fine = (squares - coarse.astype(F32)).astype(BF16)
        mean = jnp.dot(coarse, weights, preferred_element_type=F32) + jnp.dot(
            fine, weights, preferred_element_type=F32
        )
        repeats = raw.shape[1] // HEAD_DIM
        gain = gain if repeats == 1 else jnp.concatenate([gain] * repeats, axis=1)
        return (raw * lax.rsqrt(mean + EPS) * gain).astype(BF16)

    def build_tables():
        query_col = lax.broadcasted_iota(jnp.int32, (GRID_W, 128), 0)
        key_col = lax.rem(lax.broadcasted_iota(jnp.int32, (GRID_W, 128), 1), GRID_W)
        offset = key_col - query_col + WIN_COLS // 2
        band = (offset >= 0) & (offset < WIN_COLS)
        heads = head_width // HEAD_DIM
        tiles = KEYS // 128
        lines[...] = jnp.zeros_like(lines)
        for layer in range(layers):
            for head in range(heads):
                lines[:, 0:WIN_COLS] = bias_ref[layer, head]
                left = lines[...]
                right = pltpu.roll(left, GRID_W, 1)
                for tile in range(tiles):
                    j = 2 * tile
                    line = left[j : j + 1, :] + right[j + 1 : j + 2, :]
                    line = jnp.broadcast_to(line, (GRID_W, 128))
                    line = pltpu.roll(line, 128 - WIN_COLS // 2, 1, stride=1, stride_axis=0)
                    table[
                        layer,
                        head * GRID_W : (head + 1) * GRID_W,
                        tile * 128 : (tile + 1) * 128,
                    ] = jnp.where(band, line, NEG)

    def build_masks():
        own = doc_ref[...]
        every = jnp.concatenate([marks[0], own, marks[1]], axis=1).astype(F32)
        own_rows = jnp.broadcast_to(own.astype(F32), (128, tokens)).T
        base = tokens - LOW
        for row in range(rows):
            left = base + row * GRID_W
            keys_here = every[:, left : left + KEYS]
            queries_here = own_rows[row * GRID_W : (row + 1) * GRID_W, 0:1]
            maskbuf[row] = jnp.where(queries_here == keys_here, 0.0, NEG)

    lane = lax.broadcasted_iota(jnp.int32, (GRID_W, group), 1)

    def attend(layer, g, wanted):
        for row in wanted:
            low = row * GRID_W
            cols = slice(g * group, (g + 1) * group)
            q = qbuf[low : low + GRID_W, cols]
            if per_group == 2:
                zero = jnp.zeros_like(q)
                q = jnp.concatenate(
                    [
                        jnp.where(lane < HEAD_DIM, q, zero),
                        jnp.where(lane >= HEAD_DIM, q, zero),
                    ],
                    axis=0,
                )
            k = kvbuf[layer, g, low : low + KEYS, 0:group]
            v = kvbuf[layer, g, low : low + KEYS, group:]
            scores = lax.dot_general(
                q, k, (((1,), (1,)), ((), ())), preferred_element_type=F32
            )
            exps, sums = [], []
            for i in range(per_group):
                head = g * per_group + i
                s = (
                    scores[i * GRID_W : (i + 1) * GRID_W]
                    + table[layer, head * GRID_W : (head + 1) * GRID_W, :]
                    + maskbuf[row]
                )
                e = jnp.exp(s - jnp.max(s, axis=-1, keepdims=True))
                sums.append(jnp.sum(e, axis=-1, keepdims=True))
                exps.append(e.astype(BF16))
            weights = exps[0] if per_group == 1 else jnp.concatenate(exps, axis=0)
            mixed = jnp.dot(weights, v, preferred_element_type=F32)
            parts = [
                mixed[i * GRID_W : (i + 1) * GRID_W] / sums[i] for i in range(per_group)
            ]
            result = (
                parts[0] if per_group == 1 else jnp.where(lane < HEAD_DIM, parts[0], parts[1])
            )
            att[layer, mine, low : low + GRID_W, cols] = result.astype(BF16)

    chunk = 512
    for layer in range(layers):
        source = stream_ref if layer == 0 else hbuf
        target = out_ref if layer == layers - 1 else hbuf

        block = 32

        def norm_rows(i, carry):
            at = pl.ds(pl.multiple_of(i * block, block), block)
            x = source[at, :].astype(F32)
            inverse = lax.rsqrt(jnp.mean(x * x, axis=-1, keepdims=True) + EPS)
            nbuf[at, :] = (x * inverse * norm_gain_ref[layer : layer + 1, :]).astype(BF16)
            return carry

        lax.fori_loop(0, tokens // block, norm_rows, 0)

        k_gain = k_gain_ref[layer : layer + 1, :]
        q_gain = q_gain_ref[layer : layer + 1, :] * HEAD_DIM ** (-0.5)

        for g in range(groups):
            wkv_copy(layer, g, 0).wait()
            wkv_copy(layer, g, 1).wait()
            if layer == 0 and g == 0:
                wq_copy(0).start()
                wo_copy(0).start()
            own = slice(LOW, LOW + tokens)
            if paired:
                raw = jnp.dot(nbuf[...], wkvbuf[layer, g], preferred_element_type=F32)
                k_raw, v_raw = raw[:, 0:group], raw[:, group:]
            else:
                k_raw = jnp.dot(nbuf[...], wkvbuf[layer, 0], preferred_element_type=F32)
                v_raw = jnp.dot(nbuf[...], wkvbuf[layer, 1], preferred_element_type=F32)
            kvbuf[layer, g, own, 0:group] = head_norm(k_raw, k_gain)
            kvbuf[layer, g, own, group:] = v_raw.astype(BF16)
            if layer == 0 and g == 0:
                degree = has_prev.astype(jnp.int32) + has_next.astype(jnp.int32) + (tp_size - 1)
                pl.semaphore_wait(barrier, degree)
                start_both(mark_copies())
            start_both(halo(layer, g))

        if layer == 0:
            for later in range(1, layers):
                for g in range(groups):
                    wkv_copy(later, g, 0).start()
                    wkv_copy(later, g, 1).start()
                wq_copy(later).start()
                wo_copy(later).start()

        wq_copy(layer).wait()
        for start in range(0, head_width, span):
            cols = slice(start, start + span)
            raw = jnp.dot(nbuf[...], wqbuf[layer, :, cols], preferred_element_type=F32)
            qbuf[:, cols] = head_norm(raw, q_gain)
        if layer == 0:
            build_tables()
            wait_low(mark_copies())
            wait_high(mark_copies())
            build_masks()

        def attend_group(g):
            copies = halo(layer, g)
            wait_low(copies)
            attend(layer, g, range(0, 1))
            wait_high(copies)
            attend(layer, g, range(1, rows))
            for step in range(1, tp_size):
                att_copy(layer, g, step).start()

        def add_part(step, part, first, last):
            owner = lax.rem(mine + tp_size - step, tp_size)
            size = len(part) * group
            inner = slice(part[0] * group, part[0] * group + size)
            begin = owner * head_width + part[0] * group
            at = pl.ds(pl.multiple_of(begin, HEAD_DIM), size)
            if step > 0:
                for g in part:
                    att_copy(layer, g, step).wait_recv()
            for start in range(0, width, chunk):
                cols = slice(start, start + chunk)
                total = jnp.dot(
                    att[layer, owner, :, inner],
                    wobuf[layer, at, cols],
                    preferred_element_type=F32,
                )
                total += source[:, cols].astype(F32) if first else acc[:, cols]
                if last:
                    target[:, cols] = total.astype(BF16)
                else:
                    acc[:, cols] = total

        every = list(range(groups))
        half = groups // 2
        parts = [every[:half], every[half:]] if half else [every]
        pending = []
        for index, part in enumerate(parts):
            for g in part:
                attend_group(g)
                for job in pending:
                    add_part(*job)
                pending = []
            if index == 0:
                wo_copy(layer).wait()
            final = index == len(parts) - 1
            add_part(0, part, index == 0, final and tp_size == 1)
            pending = [
                (step, part, False, final and step == tp_size - 1)
                for step in range(1, tp_size)
            ]
        for job in pending:
            add_part(*job)

    wait_send_both(mark_copies())
    for layer in range(layers):
        for g in range(groups):
            wait_send_both(halo(layer, g))
            for step in range(1, tp_size):
                att_copy(layer, g, step).wait_send()


def on_device(
    sp_size,
    tp_size,
    stream,
    doc_ids,
    norm_gain,
    w_query,
    w_key,
    w_value,
    query_gain,
    key_gain,
    offset_bias,
    w_output,
):
    tokens, width = stream.shape
    layers, _, head_width = w_query.shape
    heads = head_width // HEAD_DIM
    rows = tokens // GRID_W
    all_width = w_output.shape[1]
    group = min(128, head_width)
    groups = head_width // group
    vmem = pl.BlockSpec(memory_space=pltpu.VMEM)
    hbm = pl.BlockSpec(memory_space=pl.ANY)
    sem = pltpu.SemaphoreType.DMA
    peers = max(1, tp_size - 1)
    return pl.pallas_call(
        functools.partial(kernel, sp_size, tp_size),
        out_shape=jax.ShapeDtypeStruct((tokens, width), BF16),
        in_specs=[vmem, vmem, vmem, hbm, hbm, hbm, vmem, vmem, vmem, hbm],
        out_specs=vmem,
        scratch_shapes=[
            pltpu.VMEM((layers, width, head_width), BF16),
            pltpu.VMEM(
                (layers, groups, width, 256) if group == 128 else (layers, 2, width, group), BF16
            ),
            pltpu.VMEM((layers, all_width, width), BF16),
            pltpu.VMEM((tokens, width), BF16),
            pltpu.VMEM((tokens, width), BF16),
            pltpu.VMEM((tokens, head_width), BF16),
            pltpu.VMEM((layers, groups, LOW + tokens + HIGH, 2 * group), BF16),
            pltpu.VMEM((layers, tp_size, tokens, head_width), BF16),
            pltpu.VMEM((tokens, width), F32),
            pltpu.VMEM((layers, heads * GRID_W, KEYS), F32),
            pltpu.VMEM((rows, GRID_W, KEYS), F32),
            pltpu.VMEM((2, 1, tokens), jnp.int32),
            pltpu.VMEM((WIN_ROWS, 128), F32),
            sem((layers,)),
            sem((layers, groups, 2)),
            sem((layers,)),
            sem((2,)),
            sem((2,)),
            sem((layers, groups, 2)),
            sem((layers, groups, 2)),
            sem((layers, peers, groups)),
            sem((layers, peers, groups)),
        ],
        compiler_params=pltpu.CompilerParams(
            collective_id=0, has_side_effects=True, vmem_limit_bytes=60 * 1024 * 1024
        ),
    )(
        stream,
        doc_ids.reshape(1, tokens),
        norm_gain,
        w_query,
        w_key,
        w_value,
        query_gain,
        key_gain,
        offset_bias,
        w_output,
    )


def solution(mesh):
    return jax.shard_map(
        functools.partial(on_device, mesh.shape["sp"], mesh.shape["tp"]),
        mesh=mesh,
        in_specs=(
            P("sp", None),
            P("sp"),
            P(),
            P(None, None, "tp"),
            P(None, None, "tp"),
            P(None, None, "tp"),
            P(),
            P(),
            P(None, "tp", None, None),
            P(),
        ),
        out_specs=P("sp", None),
        check_vma=False,
    )
```

time: 54 us -> 46 us (0.85)
  local copies, waits for them, and re-layouts: 6.53 us -> 2.3 us
  Pallas kernels: 47.1 us -> 43.6 us
    pallas_call x1, Pallas kernels: 47.1 us -> 43.6 us  [on_device(): pl.pallas_call(functools.partial(kernel, sp_size, tp_size), out_shape=jax...]
    another operation x4 -> x0, local copies, waits for them, and re-layouts: 2.69 us -> none  [the longest x2 1.35 us: on_device(): jnp.tile(key_gain, (1, heads))]
    pad x1 -> x0, local copies, waits for them, and re-layouts: 0.85 us -> none  [on_device(): jnp.pad(offset_bias, ((0, 0), (0, 0), (0, 0), (0, GRID_W - WIN_COLS)))]
    reshape x1 -> x0, local copies, waits for them, and re-layouts: 0.69 us -> none  [on_device(): bias = bias.reshape(layers * heads * (KEYS // 128), 128)]
where the time goes in v2:
time: 46 us; the launch traced here: 45.9 us
  Pallas kernels  43.6 us (95%)
  local copies, waits for them, and re-layouts  2.3 us (5%)
    pallas_call x1, Pallas kernels, on_device(): pl.pallas_call(functools.partial(kernel, sp_size, tp_size), out_shape=jax...  43.6 us
    unnamed x1, local copies, waits for them, and re-layouts  2.3 us

profile of v2, /device:TPU:10, one launch (start us, length us, event | category | flops | bytes accessed | tf_op | source)
XLA Modules:
  0.0 45.9 jit_solution(8521964891289527167)
XLA Ops:
  0.0 43.6 %shard_map.100 = bf16[256,2048]{1,0:T(8,128)(2,1)} custom-call(bf16[256,2048]{1,0:T(8,128)(2,1)} %stream_ref.1, s32[1,256]{1,0:T(1,128)} %bitcast.1, f32[2,2048]{1,0:T(2,128)} %norm_gain_ref.1, bf16[2,2048,512]{2,1,0:T(8,128)(2,1)} %wq_hbm.1, bf16[2,2048,512]{2,1,0:T(8,128)(2,1)} %wk_hbm.1, bf16[2,2048,512]{2,1,0:T(8,128)(2,1)} %wv_hbm.1, ...), custom_call_target="tpu_custom_call" | custom-call | tf_op jit(solution)/shard_map/pallas_call | solution.py:442
  43.6 2.3 %copy.12 = bf16[256,2048]{1,0:T(8,128)(2,1)} copy(bf16[256,2048]{1,0:T(8,128)(2,1)} %shard_map.100) | data formatting | bytes 2097152

commit v3 on v2

--- a/solution.py
+++ b/solution.py
@@ -177,9 +177,7 @@
             pair[1].wait_recv()
 
     def att_copy(layer, g, step):
-        block = att.at[layer, mine]
-        if paired:
-            block = block.at[:, pl.ds(g * group, group)]
+        block = att.at[layer, mine, g]
         return pltpu.make_async_remote_copy(
             src_ref=block,
             dst_ref=block,
@@ -256,9 +254,10 @@
     lane = lax.broadcasted_iota(jnp.int32, (GRID_W, group), 1)
 
     def attend(layer, g, wanted):
+        cols = slice(g * group, (g + 1) * group)
+        scores, weights, sums = {}, {}, {}
         for row in wanted:
             low = row * GRID_W
-            cols = slice(g * group, (g + 1) * group)
             q = qbuf[low : low + GRID_W, cols]
             if per_group == 2:
                 zero = jnp.zeros_like(q)
@@ -270,30 +269,34 @@
                     axis=0,
                 )
             k = kvbuf[layer, g, low : low + KEYS, 0:group]
-            v = kvbuf[layer, g, low : low + KEYS, group:]
-            scores = lax.dot_general(
+            scores[row] = lax.dot_general(
                 q, k, (((1,), (1,)), ((), ())), preferred_element_type=F32
             )
-            exps, sums = [], []
+        for row in wanted:
+            exps = []
+            sums[row] = []
             for i in range(per_group):
                 head = g * per_group + i
                 s = (
-                    scores[i * GRID_W : (i + 1) * GRID_W]
+                    scores[row][i * GRID_W : (i + 1) * GRID_W]
                     + table[layer, head * GRID_W : (head + 1) * GRID_W, :]
                     + maskbuf[row]
                 )
                 e = jnp.exp(s - jnp.max(s, axis=-1, keepdims=True))
-                sums.append(jnp.sum(e, axis=-1, keepdims=True))
+                sums[row].append(jnp.sum(e, axis=-1, keepdims=True))
                 exps.append(e.astype(BF16))
-            weights = exps[0] if per_group == 1 else jnp.concatenate(exps, axis=0)
-            mixed = jnp.dot(weights, v, preferred_element_type=F32)
+            weights[row] = exps[0] if per_group == 1 else jnp.concatenate(exps, axis=0)
+        for row in wanted:
+            low = row * GRID_W
+            v = kvbuf[layer, g, low : low + KEYS, group:]
+            mixed = jnp.dot(weights[row], v, preferred_element_type=F32)
             parts = [
-                mixed[i * GRID_W : (i + 1) * GRID_W] / sums[i] for i in range(per_group)
+                mixed[i * GRID_W : (i + 1) * GRID_W] / sums[row][i] for i in range(per_group)
             ]
             result = (
                 parts[0] if per_group == 1 else jnp.where(lane < HEAD_DIM, parts[0], parts[1])
             )
-            att[layer, mine, low : low + GRID_W, cols] = result.astype(BF16)
+            att[layer, mine, g, low : low + GRID_W, :] = result.astype(BF16)
 
     chunk = 512
     for layer in range(layers):
@@ -357,25 +360,25 @@
         def attend_group(g):
             copies = halo(layer, g)
             wait_low(copies)
-            attend(layer, g, range(0, 1))
             wait_high(copies)
-            attend(layer, g, range(1, rows))
+            attend(layer, g, range(rows))
             for step in range(1, tp_size):
                 att_copy(layer, g, step).start()
 
         def add_part(step, part, first, last):
             owner = lax.rem(mine + tp_size - step, tp_size)
             size = len(part) * group
-            inner = slice(part[0] * group, part[0] * group + size)
             begin = owner * head_width + part[0] * group
             at = pl.ds(pl.multiple_of(begin, HEAD_DIM), size)
             if step > 0:
                 for g in part:
                     att_copy(layer, g, step).wait_recv()
+            pieces = [att[layer, owner, g] for g in part]
+            heads_in = pieces[0] if len(pieces) == 1 else jnp.concatenate(pieces, axis=1)
             for start in range(0, width, chunk):
                 cols = slice(start, start + chunk)
                 total = jnp.dot(
-                    att[layer, owner, :, inner],
+                    heads_in,
                     wobuf[layer, at, cols],
                     preferred_element_type=F32,
                 )
@@ -454,7 +457,7 @@
             pltpu.VMEM((tokens, width), BF16),
             pltpu.VMEM((tokens, head_width), BF16),
             pltpu.VMEM((layers, groups, LOW + tokens + HIGH, 2 * group), BF16),
-            pltpu.VMEM((layers, tp_size, tokens, head_width), BF16),
+            pltpu.VMEM((layers, tp_size, groups, tokens, group), BF16),
             pltpu.VMEM((tokens, width), F32),
             pltpu.VMEM((layers, heads * GRID_W, KEYS), F32),
             pltpu.VMEM((rows, GRID_W, KEYS), F32),

time: 46 us -> 42.7 us (0.928)
  Pallas kernels: 43.6 us -> 40.2 us
    pallas_call x1, Pallas kernels: 43.6 us -> 40.2 us  [on_device(): pl.pallas_call(functools.partial(kernel, sp_size, tp_size), out_shape=jax...]
where the time goes in v3:
time: 42.7 us; the launch traced here: 42.5 us
  Pallas kernels  40.2 us (94%)
  local copies, waits for them, and re-layouts  2.3 us (5%)
    pallas_call x1, Pallas kernels, on_device(): pl.pallas_call(functools.partial(kernel, sp_size, tp_size), out_shape=jax...  40.2 us
    unnamed x1, local copies, waits for them, and re-layouts  2.3 us

profile of v3, /device:TPU:10, one launch (start us, length us, event | category | flops | bytes accessed | tf_op | source)
XLA Modules:
  0.0 42.5 jit_solution(1881741996733246664)
XLA Ops:
  0.0 40.2 %shard_map.100 = bf16[256,2048]{1,0:T(8,128)(2,1)} custom-call(bf16[256,2048]{1,0:T(8,128)(2,1)} %stream_ref.1, s32[1,256]{1,0:T(1,128)} %bitcast.1, f32[2,2048]{1,0:T(2,128)} %norm_gain_ref.1, bf16[2,2048,512]{2,1,0:T(8,128)(2,1)} %wq_hbm.1, bf16[2,2048,512]{2,1,0:T(8,128)(2,1)} %wk_hbm.1, bf16[2,2048,512]{2,1,0:T(8,128)(2,1)} %wv_hbm.1, ...), custom_call_target="tpu_custom_call" | custom-call | tf_op jit(solution)/shard_map/pallas_call | solution.py:445
  40.2 2.3 %copy.12 = bf16[256,2048]{1,0:T(8,128)(2,1)} copy(bf16[256,2048]{1,0:T(8,128)(2,1)} %shard_map.100) | data formatting | bytes 2097152

commit v4 on v3

--- a/solution.py
+++ b/solution.py
@@ -16,6 +16,7 @@
 HIGH = (WIN_ROWS - WIN_ROWS // 2 - 1) * GRID_W
 KEYS = WIN_ROWS * GRID_W
 NEG = -1e30
+CHUNK = 512
 MESH = pl.DeviceIdType.MESH
 F32 = jnp.float32
 BF16 = jnp.bfloat16
@@ -57,6 +58,7 @@
     kv_recv,
     a_send,
     a_recv,
+    out_sem,
 ):
     layers, width, head_width = wk_hbm.shape
     tokens = stream_ref.shape[0]
@@ -109,6 +111,9 @@
             device_id_type=MESH,
         )
 
+    def pieces_of(g):
+        return 2 if g == groups - 1 and rows % 2 == 0 else 1
+
     def halo(layer, g):
         here = kvbuf.at[layer, g]
         ahead = pltpu.make_async_remote_copy(
@@ -176,13 +181,16 @@
         def _():
             pair[1].wait_recv()
 
-    def att_copy(layer, g, step):
-        block = att.at[layer, mine, g]
+    def att_copy(layer, g, step, piece):
+        if pieces_of(g) == 1:
+            block = att.at[layer, mine, g]
+        else:
+            block = att.at[layer, mine, g, pl.ds(piece * (tokens // 2), tokens // 2)]
         return pltpu.make_async_remote_copy(
             src_ref=block,
             dst_ref=block,
-            send_sem=a_send.at[layer, step - 1, g],
-            recv_sem=a_recv.at[layer, step - 1, g],
+            send_sem=a_send.at[layer, step - 1, g, piece],
+            recv_sem=a_recv.at[layer, step - 1, g, piece],
             device_id={"tp": lax.rem(mine + step, tp_size)},
             device_id_type=MESH,
         )
@@ -252,6 +260,10 @@
             maskbuf[row] = jnp.where(queries_here == keys_here, 0.0, NEG)
 
     lane = lax.broadcasted_iota(jnp.int32, (GRID_W, group), 1)
+
+    def out_copy(index):
+        cols = pl.ds(index * CHUNK, CHUNK)
+        return pltpu.make_async_copy(hbuf.at[:, cols], out_ref.at[:, cols], out_sem.at[index])
 
     def attend(layer, g, wanted):
         cols = slice(g * group, (g + 1) * group)
@@ -298,10 +310,9 @@
             )
             att[layer, mine, g, low : low + GRID_W, :] = result.astype(BF16)
 
-    chunk = 512
+    chunk = CHUNK
     for layer in range(layers):
         source = stream_ref if layer == 0 else hbuf
-        target = out_ref if layer == layers - 1 else hbuf
 
         block = 32
 
@@ -361,9 +372,11 @@
             copies = halo(layer, g)
             wait_low(copies)
             wait_high(copies)
-            attend(layer, g, range(rows))
-            for step in range(1, tp_size):
-                att_copy(layer, g, step).start()
+            count = rows // pieces_of(g)
+            for piece in range(pieces_of(g)):
+                attend(layer, g, range(piece * count, (piece + 1) * count))
+                for step in range(1, tp_size):
+                    att_copy(layer, g, step, piece).start()
 
         def add_part(step, part, first, last):
             owner = lax.rem(mine + tp_size - step, tp_size)
@@ -372,7 +385,8 @@
             at = pl.ds(pl.multiple_of(begin, HEAD_DIM), size)
             if step > 0:
                 for g in part:
-                    att_copy(layer, g, step).wait_recv()
+                    for piece in range(pieces_of(g)):
+                        att_copy(layer, g, step, piece).wait_recv()
             pieces = [att[layer, owner, g] for g in part]
             heads_in = pieces[0] if len(pieces) == 1 else jnp.concatenate(pieces, axis=1)
             for start in range(0, width, chunk):
@@ -384,7 +398,9 @@
                 )
                 total += source[:, cols].astype(F32) if first else acc[:, cols]
                 if last:
-                    target[:, cols] = total.astype(BF16)
+                    hbuf[:, cols] = total.astype(BF16)
+                    if layer == layers - 1 and start > 0:
+                        out_copy(start // chunk - 1).start()
                 else:
                     acc[:, cols] = total
 
@@ -409,12 +425,16 @@
         for job in pending:
             add_part(*job)
 
+    out_copy(width // chunk - 1).start()
     wait_send_both(mark_copies())
     for layer in range(layers):
         for g in range(groups):
             wait_send_both(halo(layer, g))
             for step in range(1, tp_size):
-                att_copy(layer, g, step).wait_send()
+                for piece in range(pieces_of(g)):
+                    att_copy(layer, g, step, piece).wait_send()
+    for index in range(width // CHUNK):
+        out_copy(index).wait()
 
 
 def on_device(
@@ -446,7 +466,7 @@
         functools.partial(kernel, sp_size, tp_size),
         out_shape=jax.ShapeDtypeStruct((tokens, width), BF16),
         in_specs=[vmem, vmem, vmem, hbm, hbm, hbm, vmem, vmem, vmem, hbm],
-        out_specs=vmem,
+        out_specs=hbm,
         scratch_shapes=[
             pltpu.VMEM((layers, width, head_width), BF16),
             pltpu.VMEM(
@@ -470,8 +490,9 @@
             sem((2,)),
             sem((layers, groups, 2)),
             sem((layers, groups, 2)),
-            sem((layers, peers, groups)),
-            sem((layers, peers, groups)),
+            sem((layers, peers, groups, 2)),
+            sem((layers, peers, groups, 2)),
+            sem((width // CHUNK,)),
         ],
         compiler_params=pltpu.CompilerParams(
             collective_id=0, has_side_effects=True, vmem_limit_bytes=60 * 1024 * 1024

time: 42.7 us -> 42.4 us (level)
  no operation moved by 1% of the time
where the time goes in v4:
time: 42.4 us; the launch traced here: 42.2 us
  Pallas kernels  39.9 us (94%)
  local copies, waits for them, and re-layouts  2.3 us (5%)
    pallas_call x1, Pallas kernels, on_device(): pl.pallas_call(functools.partial(kernel, sp_size, tp_size), out_shape=jax...  39.9 us
    unnamed x1, local copies, waits for them, and re-layouts  2.3 us

profile of v4, /device:TPU:10, one launch (start us, length us, event | category | flops | bytes accessed | tf_op | source)
XLA Modules:
  0.0 42.2 jit_solution(1114507113920810442)
XLA Ops:
  0.0 39.9 %shard_map.100 = bf16[256,2048]{1,0:T(8,128)(2,1)} custom-call(bf16[256,2048]{1,0:T(8,128)(2,1)} %stream_ref.1, s32[1,256]{1,0:T(1,128)} %bitcast.1, f32[2,2048]{1,0:T(2,128)} %norm_gain_ref.1, bf16[2,2048,512]{2,1,0:T(8,128)(2,1)} %wq_hbm.1, bf16[2,2048,512]{2,1,0:T(8,128)(2,1)} %wk_hbm.1, bf16[2,2048,512]{2,1,0:T(8,128)(2,1)} %wv_hbm.1, ...), custom_call_target="tpu_custom_call" | custom-call | tf_op jit(solution)/shard_map/pallas_call | solution.py:465
  39.9 2.3 %copy.12 = bf16[256,2048]{1,0:T(8,128)(2,1)} copy(bf16[256,2048]{1,0:T(8,128)(2,1)} %shard_map.100) | data formatting | bytes 2097152

commit v5 on v4

--- a/solution.py
+++ b/solution.py
@@ -462,7 +462,7 @@
     hbm = pl.BlockSpec(memory_space=pl.ANY)
     sem = pltpu.SemaphoreType.DMA
     peers = max(1, tp_size - 1)
-    return pl.pallas_call(
+    result = pl.pallas_call(
         functools.partial(kernel, sp_size, tp_size),
         out_shape=jax.ShapeDtypeStruct((tokens, width), BF16),
         in_specs=[vmem, vmem, vmem, hbm, hbm, hbm, vmem, vmem, vmem, hbm],
@@ -509,6 +509,18 @@
         offset_bias,
         w_output,
     )
+    spec = pl.BlockSpec((tokens // 4, width), lambda i: (i, 0))
+    return pl.pallas_call(
+        pass_on,
+        grid=(4,),
+        out_shape=jax.ShapeDtypeStruct((tokens, width), BF16),
+        in_specs=[spec],
+        out_specs=spec,
+    )(result)
+
+
+def pass_on(from_ref, to_ref):
+    to_ref[...] = from_ref[...]
 
 
 def solution(mesh):

time: 42.4 us -> 43.5 us (1.026)
  Pallas kernels: 39.9 us -> 43.3 us
  local copies, waits for them, and re-layouts: 2.3 us -> 0 us
    pallas_call x0 -> x1, Pallas kernels: none -> 3.37 us  [on_device(): pl.pallas_call(pass_on, grid=(4,), out_shape=jax.ShapeDtypeStruct((tokens...]
    unnamed x1 -> x0, local copies, waits for them, and re-layouts: 2.3 us -> none
where the time goes in v5:
time: 43.5 us; the launch traced here: 43.3 us
  Pallas kernels  43.3 us (100%)
    pallas_call x1, Pallas kernels, on_device(): pl.pallas_call(functools.partial(kernel, sp_size, tp_size), out_shape=jax...  39.9 us
    pallas_call x1, Pallas kernels, on_device(): pl.pallas_call(pass_on, grid=(4,), out_shape=jax.ShapeDtypeStruct((tokens...  3.37 us

profile of v5, /device:TPU:10, one launch (start us, length us, event | category | flops | bytes accessed | tf_op | source)
XLA Modules:
  0.0 43.3 jit_solution(2752536152324250099)
XLA Ops:
  0.0 39.9 %shard_map.100.from_ref = bf16[256,2048]{1,0:T(8,128)(2,1)} custom-call(bf16[256,2048]{1,0:T(8,128)(2,1)} %stream_ref.1, s32[1,256]{1,0:T(1,128)} %bitcast.1, f32[2,2048]{1,0:T(2,128)} %norm_gain_ref.1, bf16[2,2048,512]{2,1,0:T(8,128)(2,1)} %wq_hbm.1, bf16[2,2048,512]{2,1,0:T(8,128)(2,1)} %wk_hbm.1, bf16[2,2048,512]{2,1,0:T(8,128)(2,1)} %wv_hbm.1, ...), custom_call_target="tpu_custom_call" | custom-call | tf_op jit(solution)/shard_map/pallas_call | solution.py:465
  39.9 3.4 %shard_map.101 = bf16[256,2048]{1,0:T(8,128)(2,1)} custom-call(bf16[256,2048]{1,0:T(8,128)(2,1)} %shard_map.100.from_ref), custom_call_target="tpu_custom_call" | custom-call | tf_op jit(solution)/shard_map/pallas_call | solution.py:513
